TPU v7x, 512 devices: a whole 4x8x8 slice. The times are simulated.
512 devices in a mesh: sp: 64 (over z, y), tp: 8 (over x, core).
Axes of the slice: x: 4, y: 8, z: 8, core: 2. Of those that a mesh axis runs over, the one named last changes fastest.
Arguments:
- tokens: bfloat16 [16384, 2048], P(('sp', 'tp')), may hold values from -6 to 6
- gain: float32 [2048], replicated, may hold values from 0.1 to 1.9
- w_ret_q: bfloat16 [2048, 2048], P(None, 'tp'), may hold values from -0.125 to 0.125
- w_ret_k: bfloat16 [2048, 2048], P(None, 'tp'), may hold values from -0.125 to 0.125
- w_ret_v: bfloat16 [2048, 2048], P(None, 'tp'), may hold values from -0.125 to 0.125
- w_fox_q: bfloat16 [2048, 1024], P(None, 'tp'), may hold values from -0.125 to 0.125
- w_fox_k: bfloat16 [2048, 1024], P(None, 'tp'), may hold values from -0.125 to 0.125
- w_fox_v: bfloat16 [2048, 1024], P(None, 'tp'), may hold values from -0.125 to 0.125
- fox_gates: float32 [16384, 8], P('sp', 'tp'), may hold values from -16384 to 0, as said below
- w_out_ret: bfloat16 [2048, 2048], P('tp', 'sp'), may hold values from -0.109375 to 0.109375
- w_out_fox: bfloat16 [1024, 2048], P('tp', 'sp'), may hold values from -0.109375 to 0.109375
Outputs:
- mixed: bfloat16 [16384, 2048], P(('sp', 'tp'))
Inputs may be any that keep to these rules, and one draw needn't show every extreme that they name: `fox_gates`: each head's values never rise along positions.
All inputs are finite; a program needn't handle non-finite values.
Results may differ from a plain program's by a relative error of at most 0.02.
Values may be sent and summed in bfloat16 or wider, within the bound.
No kernel may reach another device: no remote copies, remote signals or barrier semaphores. Data moves between devices by JAX's collectives and lax.ppermute only.
A program may use at most 128 MiB of HBM per device.

v0:
```python
import math

import jax
import jax.numpy as jnp
from jax import lax
from jax.sharding import Mesh
from jax.sharding import PartitionSpec as P

RET_HEADS = 8
RET_DIM = 256
FOX_DIM = 128
BLOCK = 128
SP = ("sp_0", "sp_1")
SP_TP = ("sp_0", "sp_1", "tp")


eps = 1e-06


def joined_along(pieces, dim):
    dims = list(pieces.shape[1:])
    dims[dim] *= pieces.shape[0]
    return jnp.moveaxis(pieces, 0, dim).reshape(dims)


def sent_to_all(shard, axis):
    size = lax.axis_size(axis)
    return lax.all_to_all(
        jnp.broadcast_to(shard[None], (size, *shard.shape)), axis, 0, 0, tiled=True
    )


def gathered_copies(shard, axis, dim):
    return joined_along(sent_to_all(shard, axis), dim)


def filled_with(shard, identity):
    return jax.tree.map(
        lambda part, zero: jnp.zeros_like(part) + jnp.asarray(zero, part.dtype), shard, identity
    )


def entering(shard, axes, combine, identity):
    before = start = filled_with(shard, identity)
    subtotal = shard
    for axis in reversed(axes):
        size, index = (lax.axis_size(axis), lax.axis_index(axis))
        pieces = jax.tree.map(lambda part: lax.all_gather(part, axis), subtotal)
        inside, subtotal = (start, start)
        for k in range(size):
            passed = k < index
            subtotal = combine(subtotal, jax.tree.map(lambda part: part[k], pieces))
            inside = jax.tree.map(lambda new, old: jnp.where(passed, new, old), subtotal, inside)
        before = combine(inside, before)
    return before


def side_by_side(arrays, axis, dim, along):
    widths = [a.shape[along] for a in arrays]
    both = jnp.concatenate(arrays, axis=along)
    out = lax.all_gather(both, axis, axis=dim, tiled=True)
    return tuple(jnp.split(out, [sum(widths[:k]) for k in range(1, len(widths))], axis=along))


def rows_first(arrays, axis, dims):
    turned = [jnp.moveaxis(a, dim, 0) for a, dim in zip(arrays, dims)]
    widths = [t[0].size for t in turned]
    both = jnp.concatenate([t.reshape(-1, w) for t, w in zip(turned, widths)], axis=1)
    out = lax.all_gather(both, axis, axis=0, tiled=True)
    pieces = jnp.split(out, [sum(widths[:k]) for k in range(1, len(widths))], axis=1)
    return tuple(
        (
            jnp.moveaxis(b.reshape(-1, *t.shape[1:]), 0, dim)
            for b, t, dim in zip(pieces, turned, dims)
        )
    )


def in_blocks(shard, dim, size):
    before, after = (shard.shape[:dim], shard.shape[dim + 1 :])
    return jnp.moveaxis(shard.reshape(*before, size, -1, *after), dim, 0)


def sent_and_summed(shard, axis, dim):
    size = lax.axis_size(axis)
    pieces = lax.all_to_all(in_blocks(shard, dim, size), axis, 0, 0, tiled=True)
    return jnp.sum(pieces.astype(jnp.float32), axis=0)


def head_norm(values, width):
    rows_here = values.shape[0]
    grouped = values.reshape(rows_here, -1, width)
    scaled = grouped * lax.rsqrt(jnp.mean(grouped * grouped, axis=2, keepdims=True) + eps)
    return scaled.reshape(rows_here, -1).astype(jnp.bfloat16)


def rotate(values, token_positions, width):
    rows_here = values.shape[0]
    half_width = width // 2
    inverse = 10000.0 ** (-jnp.arange(half_width, dtype=jnp.float32) / half_width)
    angles = token_positions.astype(jnp.float32)[:, None] * inverse[None, :]
    cosine = jnp.cos(angles)[:, None, :]
    sine = jnp.sin(angles)[:, None, :]
    grouped = values.astype(jnp.float32).reshape(rows_here, -1, width)
    first_half = grouped[..., :half_width]
    second_half = grouped[..., half_width:]
    turned = jnp.concatenate(
        [first_half * cosine - second_half * sine, first_half * sine + second_half * cosine],
        axis=-1,
    )
    return turned.reshape(rows_here, -1)


def decay_rates(head_ids, total):
    heads_float = head_ids.astype(jnp.float32)
    middle = RET_HEADS // 2
    fast_rate = 1.0 / (32.0 + 16.0 * heads_float)
    slow_rate = jnp.exp2(-(heads_float - middle)) / total
    return jnp.where(head_ids < middle, fast_rate, slow_rate)


def decay_tables(rates):
    offsets = jnp.arange(BLOCK, dtype=jnp.float32)
    spread = offsets[:, None] - offsets[None, :]
    causal = spread >= 0
    within = jnp.where(
        causal[None], jnp.exp(-rates[:, None, None] * jnp.where(causal, spread, 0.0)[None]), 0.0
    )
    query_decay = jnp.exp(-rates[None, :] * (offsets[:, None] + 1.0))
    key_decay = jnp.exp(-rates[None, :] * (BLOCK - 1.0 - offsets[:, None]))
    block_decay = jnp.exp(-rates * BLOCK)
    return (within, query_decay, key_decay, block_decay)


def advance(carry, key_block, value_block, key_decay, block_decay):
    scaled = (key_block.astype(jnp.float32) * key_decay[:, :, None]).astype(jnp.bfloat16)
    update = jnp.einsum("shd,she->hde", scaled, value_block, preferred_element_type=jnp.float32)
    return carry * block_decay[:, None, None] + update


def retention_blocks(queries, keys, values, rates, state, heads):
    within, query_decay, key_decay, block_decay = decay_tables(rates)
    count = queries.shape[0] // BLOCK

    def shaped(array):
        return array.reshape(count, BLOCK, heads, RET_DIM)

    def step(carry, blocks):
        query_block, key_block, value_block = blocks
        scores = (
            jnp.einsum("thd,shd->hts", query_block, key_block, preferred_element_type=jnp.float32)
            * within
        )
        inner = jnp.einsum(
            "hts,she->the",
            scores.astype(jnp.bfloat16),
            value_block,
            preferred_element_type=jnp.float32,
        )
        cross = (
            jnp.einsum("thd,hde->the", query_block.astype(jnp.float32), carry)
            * query_decay[:, :, None]
        )
        return (advance(carry, key_block, value_block, key_decay, block_decay), inner + cross)

    final_state, outputs = lax.scan(step, state, (shaped(queries), shaped(keys), shaped(values)))
    return (final_state, outputs.reshape(count * BLOCK, heads * RET_DIM))


def join_states(earlier, later):
    return (earlier[0] * later[0], earlier[1] * later[0][:, None, None] + later[1])


def fox_weights(queries, keys, query_gates, key_gates, query_pos, key_pos):
    scores = jnp.einsum(
        "qhd,khd->hqk", queries, keys, preferred_element_type=jnp.float32
    ) * FOX_DIM ** (-0.5)
    scores = scores + query_gates.T[:, :, None] - key_gates.T[:, None, :]
    allowed = key_pos[None, :] <= query_pos[:, None]
    return jnp.exp(jnp.where(allowed[None], scores, -jnp.inf))


def add_block(numer, denom, weights, values):
    numer = numer + jnp.einsum(
        "hqk,khd->qhd", weights.astype(jnp.bfloat16), values, preferred_element_type=jnp.float32
    )
    denom = denom + jnp.sum(weights, axis=2).T
    return (numer, denom)


def per_device(
    tokens,
    gain,
    w_ret_q,
    w_ret_k,
    w_ret_v,
    w_fox_q,
    w_fox_k,
    w_fox_v,
    fox_gates,
    w_out_ret,
    w_out_fox,
):
    inputs = tokens.astype(jnp.float32)
    normed = (
        inputs * lax.rsqrt(jnp.mean(inputs * inputs, axis=1, keepdims=True) + eps) * gain
    ).astype(jnp.bfloat16)
    weights_in = (w_ret_q, w_ret_k, w_ret_v, w_fox_q, w_fox_k, w_fox_v)
    piece = gathered_copies(normed, "tp", 0)
    products = [jnp.dot(piece, matrix, preferred_element_type=jnp.float32) for matrix in weights_in]
    projected = jnp.concatenate(products, axis=1).astype(jnp.bfloat16)
    ret_width = w_ret_q.shape[1]
    fox_width = w_fox_q.shape[1]
    edges = [
        0,
        ret_width,
        2 * ret_width,
        3 * ret_width,
        3 * ret_width + fox_width,
        3 * ret_width + 2 * fox_width,
        3 * ret_width + 3 * fox_width,
    ]
    pieces_out = [projected[:, edges[column] : edges[column + 1]] for column in range(6)]
    ret_query, ret_key, ret_value, fox_query, fox_key, fox_value = pieces_out
    length = projected.shape[0]
    sp_count = lax.axis_size(SP)
    total = length * sp_count
    offset = lax.axis_index(SP) * length
    token_positions = offset + jnp.arange(length, dtype=jnp.int32)
    ret_heads = ret_width // RET_DIM
    fox_heads = fox_width // FOX_DIM
    head_ids = lax.axis_index("tp") * ret_heads + jnp.arange(ret_heads, dtype=jnp.int32)
    rates = decay_rates(head_ids, float(total))
    query_rot = rotate(ret_query, token_positions, RET_DIM).astype(jnp.bfloat16)
    key_rot = (rotate(ret_key, token_positions, RET_DIM) * RET_DIM ** (-0.5)).astype(jnp.bfloat16)
    span_decay = jnp.exp(-rates * length)
    empty_state = jnp.zeros((ret_heads, RET_DIM, RET_DIM), jnp.float32)
    identity = (jnp.ones_like(span_decay), empty_state)
    final_state, local_part = retention_blocks(
        query_rot, key_rot, ret_value, rates, empty_state, ret_heads
    )
    carried = entering((span_decay, final_state), SP, join_states, identity)[1]
    query_up = query_rot.astype(jnp.float32).reshape(length, ret_heads, RET_DIM)
    steps_in = jnp.arange(length, dtype=jnp.float32)
    reach = jnp.exp(-rates[None, :] * (steps_in[:, None] + 1.0))
    carried_part = jnp.einsum("thd,hde->the", query_up, carried) * reach[:, :, None]
    ret_raw = local_part + carried_part.reshape(length, ret_width)
    ret_mixed = head_norm(ret_raw, RET_DIM)
    gates_all = gathered_copies(fox_gates, SP, 0)
    query3 = fox_query.reshape(length, fox_heads, FOX_DIM)
    zero_numer = jnp.zeros((length, fox_heads, FOX_DIM), jnp.float32)
    zero_denom = jnp.zeros((length, fox_heads), jnp.float32)
    last_query = offset + length - 1
    keys, values = side_by_side((fox_key, fox_value), SP, 0, 1)
    rows_here = keys.shape[0]
    width = math.gcd(rows_here, 512)

    def one_block(state, index):
        begin = index * width

        def compute(accum):
            key_block = lax.dynamic_slice_in_dim(keys, begin, width, 0).reshape(
                width, fox_heads, FOX_DIM
            )
            value_block = lax.dynamic_slice_in_dim(values, begin, width, 0).reshape(
                width, fox_heads, FOX_DIM
            )
            key_gates = lax.dynamic_slice_in_dim(gates_all, begin, width, 0)
            key_pos = begin + jnp.arange(width, dtype=jnp.int32)
            weights = fox_weights(query3, key_block, fox_gates, key_gates, token_positions, key_pos)
            return add_block(accum[0], accum[1], weights, value_block)

        def skip(accum):
            return accum

        return (lax.cond(begin <= last_query, compute, skip, state), None)

    result, _ = lax.scan(
        one_block, (zero_numer, zero_denom), jnp.arange(rows_here // width, dtype=jnp.int32)
    )
    numer, denom = result
    fox_raw = (numer / denom[:, :, None]).reshape(length, fox_width)
    fox_mixed = head_norm(fox_raw, FOX_DIM)
    out_ret, out_fox = rows_first((w_out_ret, w_out_fox), SP, (1, 1))
    summed = sent_and_summed(
        (
            jnp.dot(ret_mixed, out_ret, preferred_element_type=jnp.float32)
            + jnp.dot(fox_mixed, out_fox, preferred_element_type=jnp.float32)
        ).astype(jnp.bfloat16),
        "tp",
        0,
    )
    return summed.astype(jnp.bfloat16)


def solution(mesh):
    split = Mesh(mesh.devices.reshape(8, 8, mesh.shape["tp"]), ("sp_0", "sp_1", "tp"))
    return jax.shard_map(
        per_device,
        mesh=split,
        in_specs=(
            P(SP_TP, None),
            P(),
            P(None, "tp"),
            P(None, "tp"),
            P(None, "tp"),
            P(None, "tp"),
            P(None, "tp"),
            P(None, "tp"),
            P(SP, "tp"),
            P("tp", SP),
            P("tp", SP),
        ),
        out_specs=P(SP_TP, None),
        check_vma=False,
    )
```

profile of v0, /device:TPU:496, one launch (start us, length us, event | category | flops | bytes accessed | tf_op | source)
XLA Modules:
  0.0 491.8 jit_solution(2575343854345460355)
XLA Ops:
  9.8 4.3 all-to-all-start
  14.3 15.7 %all-to-all-done = bf16[8,32,2048]{2,1,0:T(8,128)(2,1)S(1)} async-done(((bf16[8,32,2048]{2,1,0:T(8,128)(2,1)}), bf16[8,32,2048]{2,1,0:T(8,128)(2,1)S(1)}, u32[]{:S(2)}, u32[]{:S(2)}) %all-to-all-start) | async-done | bytes 1048608 | tf_op jit(solution)/shard_map/all_to_all | solution.py:28
  33.7 7.6 %while.29 = (s32[]{:T(128)}, f32[1,256,256]{2,1,0:T(8,128)S(1)}, f32[2,128,1,256]{1,0,3,2:T(2,128)S(1)}, f32[1]{0:T(128)}, bf16[2,128,1,256]{3,1,2,0:T(8,128)(2,...) while((s32[]{:T(128)}, f32[1,256,256]{2,1,0:T(8,128)S(1)}, ...), condition=%wide.region_2.3_spmd.clone.clone.clone, body=%wide.region_1.2_spmd.clone.clone.clone.sunk | while | flops 50872832 | bytes 1840267 | solution.py:166
  34.3 2.9 dynamic_update_slice.8
  38.1 2.9 dynamic_update_slice.8
  44.1 14.3 %all-reduce = f32[8]{0:T(128)S(1)} all-reduce(f32[8]{0:T(128)S(1)} %dynamic-update-slice), channel_id=2, replica_groups=mesh['sp_0'=8,'sp_1'=8,'tp'=8] {'sp_1'}, use_global_device_ids=true, to_apply=%add | all-reduce | flops 8 | bytes 64
  60.9 20.0 %all-gather.14.cloned.1.call-done = f32[8,256,256]{2,1,0:T(8,128)} async-done(((f32[1,256,256]{2,1,0:T(8,128)}), f32[8,256,256]{2,1,0:T(8,128)}) %all-gather.14.cloned.1.call-update) | async-done | bytes 2097168 | tf_op jit(solution)/shard_map/all_gather | solution.py:48
  80.9 6.7 %bitcast_add_fusion.4 = f32[1,1,256,256]{3,2,1,0:T(8,128)} fusion(f32[8,256,256]{2,1,0:T(8,128)} %all-gather.14.cloned.1.call-done, f32[]{:T(128)} %bitcast.32, f32[]{:T(128)} %bitcast.30, f32[]{:T(128)} %bitcast.28, f32[]{:T(128)} %bitcast.26, f32[]{:T(128)} %bitcast.24, f32[]{:T(128)} %bitcast.23, f32[]{:T(128)} %bitcast.22, f32[]{:T(128)} %bitcast.21), kind=kLoop, calls=%fused_computation.120 | loop fusion | flops 983040 | bytes 2359328 | tf_op jit(solution)/shard_map/add | solution.py:171
  94.7 11.7 %all-to-all-start.1 = ((f32[64,256,1]{1,2,0:T(1,128)}), f32[64,256,1]{1,2,0:T(1,128)S(1)}, u32[]{:S(2)}, u32[]{:S(2)}) async-start(f32[64,256,1]{1,2,0:T(1,128)} %broadcast_in_dim.33), calls=%async_computation.1 | async-start | bytes 131072 | tf_op jit(solution)/shard_map/all_to_all | solution.py:28
  106.4 15.3 %all-reduce.1 = f32[8]{0:T(128)S(1)} all-reduce(f32[8]{0:T(128)S(1)} %dynamic-update-slice.1), channel_id=3, replica_groups=mesh['sp_0'=8,'sp_1'=8,'tp'=8] {'sp_0'}, use_global_device_ids=true, to_apply=%add.1 | all-reduce | flops 8 | bytes 64
  131.2 11.3 %multiply_reduce_fusion = (f32[256]{0:T(256)S(1)}, f32[256,1,256]{0,2,1:T(8,128)S(1)}) fusion(f32[256,1,256]{0,2,1:T(8,128)S(1)} %reshape.652, f32[256]{0:T(256)S(1)} %multiply_exponential_fusion, bf16[256,128]{0,1:T(8,128)(2,1)S(1)} %bitcast.300, bf16[256,128]{0,1:T(8,128)(2,1)S(1)} %bitcast.299, f32[8,1,256,256]{3,2,1,0:T(8,128)} %all-gather.8.cloned.1.call-done, ...), kind=kOutput, calls=%fused_computation.139 | convolution fusion | flops 37224192 | bytes 4851796 | tf_op jit(solution)/shard_map/thd,hde->the/dot_general | solution.py:246
  142.5 71.0 %all-gather.10.cloned.1.call-done = bf16[2048,384]{1,0:T(8,128)(2,1)} async-done(((bf16[32,384]{1,0:T(8,128)(2,1)}), bf16[2048,384]{1,0:T(8,128)(2,1)}) %all-gather.10.cloned.1.call-update) | async-done | bytes 1572880 | tf_op jit(solution)/shard_map/all_gather | solution.py:69
  213.5 3.1 fusion.72
  216.6 105.2 %all-gather.12.cloned.1.call-done = bf16[16384,256]{0,1:T(8,128)(2,1)} async-done(((bf16[256,256]{0,1:T(8,128)(2,1)}), bf16[16384,256]{0,1:T(8,128)(2,1)}) %all-gather.12.cloned.1.call-update) | async-done | bytes 8388624 | tf_op jit(solution)/shard_map/all_gather | solution.py:61
  321.8 5.8 %fusion.177 = (bf16[16384,128]{0,1:T(8,128)(2,1)}, bf16[16384,128]{0,1:T(8,128)(2,1)}) fusion(bf16[16384,256]{0,1:T(8,128)(2,1)} %all-gather.12.cloned.1.call-done), kind=kLoop, calls=%fused_computation.228 | loop fusion | bytes 16777216 | tf_op jit(solution)/shard_map/split | solution.py:62
  327.6 6.4 %copy.33 = bf16[16384,128]{1,0:T(8,128)(2,1)} copy(bf16[16384,128]{0,1:T(8,128)(2,1)} %get-tuple-element.367) | data formatting | bytes 8388608
  334.0 6.4 %copy.32 = bf16[16384,128]{1,0:T(8,128)(2,1)} copy(bf16[16384,128]{0,1:T(8,128)(2,1)} %get-tuple-element.368) | data formatting | bytes 8388608
  340.4 121.7 %while.28 = (s32[]{:T(128)}, f32[256,1,128]{0,2,1:T(8,128)S(1)}, f32[256,1]{0,1:T(1,128)S(1)}, s32[32]{0:T(128)S(1)}, s32[]{:T(128)}, /*index=5*/bf16[16384,128]...) while((s32[]{:T(128)}, f32[256,1,128]{0,2,1:T(8,128)S(1)}, ...), condition=%wide.region_8.9_spmd.clone, body=%wide.region_4.8_spmd.clone.sunk | while | flops 68059904 | bytes 1133913 | solution.py:278
  353.1 2.5 conditional.3
  356.9 2.5 conditional.3
  368.3 2.5 conditional.3
  372.1 2.5 conditional.3
  383.5 2.5 conditional.3
  464.5 20.0 %all_to_all.15 = bf16[8,32,2048]{2,1,0:T(8,128)(2,1)S(1)} all-to-all(bf16[8,32,2048]{2,1,0:T(8,128)(2,1)S(1)} %bitcast.298), channel_id=1, replica_groups=mesh['sp_0'=8,'sp_1'=8,'tp'=8] {'tp'}, dimensions={0} | all-to-all | bytes 2097152 | tf_op jit(solution)/shard_map/all_to_all | solution.py:86
  (360 shorter events, 193.8 us)
Async XLA Ops:
  6.5 23.5 %copy-start = (bf16[2048,256]{1,0:T(8,128)(2,1)S(1)}, bf16[2048,256]{1,0:T(8,128)(2,1)}, u32[]{:S(2)}) copy-start(bf16[2048,256]{1,0:T(8,128)(2,1)} %param.21) | copy-start | bytes 3145732
  9.8 20.2 %all-to-all-start = ((bf16[8,32,2048]{2,1,0:T(8,128)(2,1)}), bf16[8,32,2048]{2,1,0:T(8,128)(2,1)S(1)}, u32[]{:S(2)}, u32[]{:S(2)}) async-start(bf16[8,32,2048]{2,1,0:T(8,128)(2,1)} %broadcast_in_dim.28), calls=%async_computation | async-start | bytes 2097152 | tf_op jit(solution)/shard_map/all_to_all | solution.py:28
  14.1 66.8 %all-gather.14.cloned.1.call-start = ((), (), s32[]{:S(2)}) async-start(), calls=%async_computation.6 | async-start | bytes 2359296 | tf_op jit(solution)/shard_map/all_gather | solution.py:48
  30.0 2.2 copy-start.2
  41.3 0.7 copy-start.1
  41.3 39.6 %copy-start.6 = (f32[2,128,1,256]{1,0,3,2:T(2,128)}, f32[2,128,1,256]{1,0,3,2:T(2,128)S(1)}, u32[]{:S(2)}) copy-start(f32[2,128,1,256]{1,0,3,2:T(2,128)S(1)} %get-tuple-element.149) | copy-start | bytes 786436
  41.3 46.4 %copy-start.7 = (bf16[256,32]{0,1:T(8,128)(2,1)S(1)}, bf16[256,32]{0,1:T(8,128)(2,1)}, u32[]{:S(2)}) copy-start(bf16[256,32]{0,1:T(8,128)(2,1)} %param.26) | copy-start | bytes 49156
  41.3 47.8 %copy-start.3 = (bf16[2048,128]{1,0:T(8,128)(2,1)S(1)}, bf16[2048,128]{1,0:T(8,128)(2,1)}, u32[]{:S(2)}) copy-start(bf16[2048,128]{1,0:T(8,128)(2,1)} %param.24) | copy-start | bytes 1572868
  42.0 89.2 %all-gather.8.cloned.1.call-start = ((), (), s32[]{:S(2)}) async-start(), calls=%async_computation.3 | async-start | bytes 2359296 | tf_op jit(solution)/shard_map/all_gather | solution.py:48
  80.9 8.6 %copy-start.4 = (bf16[2048,128]{1,0:T(8,128)(2,1)S(1)}, bf16[2048,128]{1,0:T(8,128)(2,1)}, u32[]{:S(2)}) copy-start(bf16[2048,128]{1,0:T(8,128)(2,1)} %param.23) | copy-start | bytes 1572868
  87.6 125.9 %all-gather.10.cloned.1.call-start = ((), (), s32[]{:S(2)}) async-start(), calls=%async_computation.4 | async-start | bytes 1597440 | tf_op jit(solution)/shard_map/all_gather | solution.py:69
  89.0 232.8 %all-gather.12.cloned.1.call-start = ((), (), s32[]{:S(2)}) async-start(), calls=%async_computation.5 | async-start | bytes 8519680 | tf_op jit(solution)/shard_map/all_gather | solution.py:61
  89.6 39.5 %copy-start.5 = (bf16[2048,128]{1,0:T(8,128)(2,1)S(1)}, bf16[2048,128]{1,0:T(8,128)(2,1)}, u32[]{:S(2)}) copy-start(bf16[2048,128]{1,0:T(8,128)(2,1)} %param.22) | copy-start | bytes 1572868
  94.7 245.7 %all-to-all-start.1 = ((f32[64,256,1]{1,2,0:T(1,128)}), f32[64,256,1]{1,2,0:T(1,128)S(1)}, u32[]{:S(2)}, u32[]{:S(2)}) async-start(f32[64,256,1]{1,2,0:T(1,128)} %broadcast_in_dim.33), calls=%async_computation.1 | async-start | bytes 131072 | tf_op jit(solution)/shard_map/all_to_all | solution.py:28
  334.0 6.5 %copy-start.8 = (f32[256,1]{0,1:T(1,128)S(1)}, f32[256,1]{0,1:T(1,128)}, u32[]{:S(2)}) copy-start(f32[256,1]{0,1:T(1,128)} %param.25) | copy-start | bytes 3076
Sparse Core Ops, SparseCore 0:
  42.1 38.7 all-gather.13
  87.7 43.3 all-gather.7
  134.2 79.2 all-gather.9
  216.3 105.3 all-gather.11
where the time goes:
time: 494 us; the launch traced here: 492 us
  waiting for transfers between devices  214 us (43%)
  matrix products  98.6 us (20%)
  local copies, waits for them, and re-layouts  55.7 us (11%)
  blocking collectives  49.6 us (10%)
  loops' own time  23.7 us (5%)
  between operations  19.7 us (4%)
  starting transfers between devices  16.1 us (3%)
  other arithmetic  14.8 us (3%)
    all_gather x1, waiting for transfers between devices, side_by_side(): out = lax.all_gather(both, axis, axis=dim, tiled=True)  105 us
    all_gather x1, waiting for transfers between devices, rows_first(): out = lax.all_gather(both, axis, axis=0, tiled=True)  71 us
    dot_general x32, matrix products, fox_weights(): jnp.einsum('qhd,khd->hqk', queries, keys, preferred_element_type=jnp.floa...  39.5 us
    dot_general x32, matrix products, add_block(): jnp.einsum('hqk,khd->qhd', weights.astype(jnp.bfloat16), values, preferre...  36.7 us
    unnamed x2, blocking collectives  29.6 us
    another operation x1, loops' own time, per_device(): lax.scan(one_block, (zero_numer, zero_denom), jnp.arange(rows_here // wid...  22.1 us
    all_gather x2, waiting for transfers between devices, entering(): pieces = jax.tree.map(lambda part: lax.all_gather(part, axis), subtotal)  21.7 us
    all_to_all x1, blocking collectives, sent_and_summed(): pieces = lax.all_to_all(in_blocks(shard, dim, size), axis, 0, 0, tiled=True)  20 us
  transfers between devices with their start and end apart: 6, of which 5 were waited for; matrix products, arithmetic and copies ran while one was open for 9% of the time, Pallas kernels for 0%

commit v1 on v0

v1 whole, which is shorter than its diff:
```python
import functools
import math

import jax
import jax.numpy as jnp
import numpy as np
from jax import lax
from jax.experimental import pallas as pl
from jax.experimental.pallas import tpu as pltpu
from jax.sharding import Mesh
from jax.sharding import PartitionSpec as P

N = 8
RUN = 256
LANES = 128
RET = 256
FOX = 128
eps = 1e-06
ALL = ("z", "y", "x", "c")
SP = ("z", "y")
TP = ("x", "c")

Q0, QG0, SA0, SB0, W0, R1 = 0, 256, 272, 336, 400, 496
K0, V0, KG0, TA0, TB0, WW0, R2 = 0, 256, 512, 528, 592, 656, 1424
N0, D0, CA0, CB0, R3 = 0, 256, 272, 336, 400

HEADS = np.arange(8, dtype=np.float64)
RATES = np.where(HEADS < 4, 1.0 / (32.0 + 16.0 * HEADS), np.exp2(-(HEADS - 4)) / 16384.0)
RATE_ROWS = np.stack([RATES, np.exp(-RATES * RUN), np.exp(-RATES * RUN * N)]).astype(np.float32)
INVERSE = 10000.0 ** (-np.arange(LANES, dtype=np.float64) / LANES)
ROW_ANGLE = np.arange(RUN, dtype=np.float64)[:, None] * INVERSE
RUN_ANGLE = (RUN * np.arange(64, dtype=np.float64))[:, None] * INVERSE
ROW_TURN = np.stack([np.cos(ROW_ANGLE), np.sin(ROW_ANGLE)]).astype(np.float32)
RUN_TURN = np.stack([np.cos(RUN_ANGLE), np.sin(RUN_ANGLE)]).astype(np.float32)

BF = jnp.bfloat16
F32 = jnp.float32


def device_id(z, y, x, c):
    return ((z * N + y) * 4 + x) * 2 + c


Y_GROUPS = [[[device_id(z, y, x, c) for y in range(N)] for z in range(N) for x in range(4)] for c in (0, 1)]
Z_GROUPS = [[[device_id(z, y, x, c) for z in range(N)] for y in range(N) for x in range(4)] for c in (0, 1)]
GROUPS_A = Y_GROUPS[0] + Z_GROUPS[1]
GROUPS_B = Z_GROUPS[0] + Y_GROUPS[1]


def exchanged(message, groups):
    return lax.all_to_all(message, ALL, 0, 0, axis_index_groups=groups, tiled=True)


def swapped(array):
    return lax.ppermute(array, "c", [(0, 1), (1, 0)])


def places():
    z, y, c = lax.axis_index("z"), lax.axis_index("y"), lax.axis_index("c")
    first = c == 0
    return z * N + y, jnp.where(first, y, z), jnp.where(first, z, y), c


def dot_nt(left, right):
    return lax.dot_general(left, right, (((1,), (1,)), ((), ())), preferred_element_type=F32)


def dot_tn(left, right):
    return lax.dot_general(left, right, (((0,), (0,)), ((), ())), preferred_element_type=F32)


def dot(left, right):
    return jnp.dot(left, right, preferred_element_type=F32)


def project_kernel(
    rates, own, other, gain, wrq, wrk, wrv, wfq, wfk, wfv, gates, wt, row_turn, run_turn,
    m1, states, kvg, qrot, inner, xs,
):
    place, _, _, c = places()
    head = lax.axis_index("x") * 2 + c
    rate = rates[0, head]
    for j in range(4):
        for part, side in ((own, c), (other, 1 - c)):
            x = part[j].astype(F32)
            scaled = x * lax.rsqrt(jnp.mean(x * x, axis=1, keepdims=True) + eps) * gain[...]
            xs[pl.ds(pl.multiple_of(64 * j + 32 * side, 32), 32), :] = scaled.astype(BF)
    x = xs[...]
    cos_run = run_turn[0, pl.ds(place, 1), :]
    sin_run = run_turn[1, pl.ds(place, 1), :]
    cosine = row_turn[0] * cos_run - row_turn[1] * sin_run
    sine = row_turn[1] * cos_run + row_turn[0] * sin_run

    def turned(values, scale):
        first, second = values[:, :LANES], values[:, LANES:]
        return jnp.concatenate(
            [(first * cosine - second * sine) * scale, (first * sine + second * cosine) * scale], axis=1
        )

    rk = turned(dot(x, wrk[...]).astype(BF).astype(F32), RET**-0.5).astype(BF)
    rv = dot(x, wrv[...]).astype(BF)
    row = lax.broadcasted_iota(jnp.int32, (RUN, RET), 0)
    col = lax.broadcasted_iota(jnp.int32, (RUN, RET), 1)
    kd = (rk.astype(F32) * jnp.exp(-rate * (RUN - 1 - row).astype(F32))).astype(BF)
    state = dot_tn(kd, rv).astype(BF)
    for j in range(N):
        for half in range(2):
            piece = state[32 * j : 32 * j + 32, LANES * half : LANES * half + LANES]
            states[j, 32 * half : 32 * half + 32, :] = piece
            m1[j, SA0 + 32 * half : SA0 + 32 * half + 32, :] = piece
            m1[j, SB0 + 32 * half : SB0 + 32 * half + 32, :] = piece
    rq = turned(dot(x, wrq[...]).astype(BF).astype(F32), 1.0).astype(BF)
    qrot[...] = rq
    spread = row - col
    within = jnp.where(spread >= 0, jnp.exp(-rate * jnp.maximum(spread, 0).astype(F32)), 0.0)
    inner[...] = dot((dot_nt(rq, rk) * within).astype(BF), rv)
    fq = dot(x, wfq[...]).astype(BF)
    kvg[K0 : K0 + RUN, :] = dot(x, wfk[...]).astype(BF)
    kvg[V0 : V0 + RUN, :] = dot(x, wfv[...]).astype(BF)
    line = lax.broadcasted_iota(jnp.int32, (16, LANES), 0)
    gate = jnp.where(line < 8, gates[0:1, :], gates[1:2, :]) * (FOX**0.5)
    high = gate.astype(BF).astype(F32)
    middle = (gate - high).astype(BF).astype(F32)
    low = gate - high - middle
    slot = line & 7
    third = jnp.where(slot == 0, high, jnp.where(slot == 1, middle, low))
    of_query = jnp.where(slot < 3, third, jnp.where(slot < 6, 1.0, 0.0)).astype(BF)
    third = jnp.where(slot == 3, high, jnp.where(slot == 4, middle, low))
    of_key = jnp.where(slot < 3, 1.0, jnp.where(slot < 6, -third, 0.0)).astype(BF)
    kvg[KG0 : KG0 + 16, :] = of_key
    for j in range(N):
        m1[j, Q0 : Q0 + RUN, :] = fq
        m1[j, QG0 : QG0 + 16, :] = of_query
        for k in range(3):
            m1[j, W0 + 32 * k : W0 + 32 * k + 32, :] = wt[k]


def totals_kernel(rates, got1, kvg, m2):
    head = lax.axis_index("x") * 2 + lax.axis_index("c")
    sums = []
    for start, which in ((SA0, head), (SB0, head ^ 1)):
        decay = rates[1, which]
        total = got1[0, start : start + 64, :].astype(F32)
        for j in range(1, N):
            total = total * decay + got1[j, start : start + 64, :].astype(F32)
        sums.append(total.astype(BF))
    for j in range(N):
        m2[j, 0 : KG0 + 16, :] = kvg[...]
        m2[j, TA0 : TA0 + 64, :] = sums[0]
        m2[j, TB0 : TB0 + 64, :] = sums[1]
        for k in range(N):
            m2[j, WW0 + 96 * k : WW0 + 96 * k + 96, :] = got1[k, W0 : W0 + 96, :]


def as_columns(rows, eye):
    lines = rows.astype(F32)
    wide = jnp.concatenate([lines[0:8], lines[8:16]], axis=1)
    wide = jnp.concatenate([wide, jnp.zeros((LANES - 8, RUN), F32)], axis=0).astype(BF)
    return dot_nt(eye, wide).astype(BF)


def attention_kernel(rates, got1, got2, m3, keys, values):
    _, a, b, c = places()
    head = lax.axis_index("x") * 2 + c
    row = lax.broadcasted_iota(jnp.int32, (RUN, RUN), 0)
    col = lax.broadcasted_iota(jnp.int32, (RUN, RUN), 1)
    eye = jnp.where(row == col, 1.0, 0.0).astype(BF)
    diagonal = (row == col)[:LANES, :LANES]
    ahead = col - row
    for i in range(N):
        keys[i, :, :LANES] = got2[i, K0 : K0 + RUN, :]
        keys[i, :, LANES:] = as_columns(got2[i, KG0 : KG0 + 16, :], eye)
        values[i, :, :LANES] = got2[i, V0 : V0 + RUN, :]
        values[i, :, LANES:] = jnp.ones((RUN, LANES), BF)

    def one_run(j, carry):
        query = jnp.concatenate(
            [got1[j, Q0 : Q0 + RUN, :], as_columns(got1[j, QG0 : QG0 + 16, :], eye)], axis=1
        )
        of_query = jnp.where(c == 0, b * N + j, j * N + b)
        total = jnp.zeros((RUN, 2 * LANES), F32)
        for i in range(N):
            of_key = jnp.where(c == 0, i * N + a, a * N + i)
            score = dot_nt(query, keys[i]) * (FOX**-0.5 * math.log2(math.e))
            score = jnp.where(ahead <= (of_query - of_key) * RUN, score, -jnp.inf)
            total = total + dot(jnp.exp2(score).astype(BF), values[i])
        m3[j, N0 : N0 + RUN, :] = total[:, :LANES].astype(BF)
        den = [
            jnp.sum(jnp.where(diagonal, total[LANES * h : LANES * h + LANES, LANES:], 0.0), axis=0, keepdims=True)
            for h in range(2)
        ]
        line = lax.broadcasted_iota(jnp.int32, (16, LANES), 0)
        den = jnp.where((line & 1) == 0, den[0], den[1])
        high = den.astype(BF).astype(F32)
        m3[j, D0 : D0 + 16, :] = jnp.where(line < 2, high, jnp.where(line < 4, den - high, 0.0)).astype(BF)
        return carry

    lax.fori_loop(0, N, one_run, 0)
    for own, (sums, slices, carried) in enumerate(((TA0, SA0, CA0), (TB0, SB0, CB0))):
        which = head ^ own
        per_run, per_row = rates[1, which], rates[2, which]
        state = jnp.zeros((64, LANES), F32)
        for k in range(N):
            state = jnp.where(k < b, state * per_row + got2[k, sums : sums + 64, :].astype(F32), state)
        for j in range(N):
            m3[j, carried : carried + 64, :] = state.astype(BF)
            state = state * per_run + got1[j, slices : slices + 64, :].astype(F32)


def output_kernel(rates, got2, got3, sent, qrot, inner, keep, give, weight, mixed, state):
    _, _, _, c = places()
    rate = rates[0, lax.axis_index("x") * 2 + c]
    for i in range(N):
        for k in range(N):
            at = pl.multiple_of(jnp.where(c == 0, i * N + k, k * N + i) * 32, 32)
            for h in range(3):
                start = WW0 + 96 * k + 32 * h
                weight[pl.ds(at, 32), LANES * h : LANES * h + LANES] = got2[i, start : start + 32, :]
    num = got3[0, N0 : N0 + RUN, :].astype(F32)
    den = got3[0, D0 : D0 + 16, :].astype(F32)
    for j in range(1, N):
        num = num + got3[j, N0 : N0 + RUN, :].astype(F32)
        den = den + got3[j, D0 : D0 + 16, :].astype(F32)
    row = lax.broadcasted_iota(jnp.int32, (LANES, LANES), 0)
    col = lax.broadcasted_iota(jnp.int32, (LANES, LANES), 1)
    for h in range(2):
        line = den[h : h + 1, :] + den[h + 2 : h + 3, :]
        column = jnp.sum(jnp.where(row == col, line, 0.0), axis=1, keepdims=True)
        raw = num[LANES * h : LANES * h + LANES] / column
        raw = raw * lax.rsqrt(jnp.mean(raw * raw, axis=1, keepdims=True) + eps)
        mixed[LANES * h : LANES * h + LANES, RET:] = raw.astype(BF)
    for j in range(N):
        for half in range(2):
            start = 32 * half
            piece = jnp.where(
                c == 0, got3[j, CA0 + start : CA0 + start + 32, :].astype(F32), sent[j, start : start + 32, :].astype(F32)
            )
            state[32 * j : 32 * j + 32, LANES * half : LANES * half + LANES] = piece.astype(BF)
    steps = lax.broadcasted_iota(jnp.int32, (RUN, RET), 0)
    raw = inner[...] + dot(qrot[...], state[...]) * jnp.exp(-rate * (steps + 1).astype(F32))
    raw = raw * lax.rsqrt(jnp.mean(raw * raw, axis=1, keepdims=True) + eps)
    mixed[:, :RET] = raw.astype(BF)
    for side, target in ((c, keep), (1 - c, give)):
        rows = jnp.concatenate(
            [mixed[pl.ds(pl.multiple_of(64 * j + 32 * side, 32), 32), :] for j in range(4)], axis=0
        )
        for n in range(4):
            part = dot_nt(rows, weight[512 * n : 512 * n + 512, :])
            for j in range(4):
                target[j, :, 512 * n : 512 * n + 512] = part[32 * j : 32 * j + 32].astype(target.dtype)


def vmem(count):
    return [pl.BlockSpec(memory_space=pltpu.VMEM)] * count


def call(kernel, outs, scratch, args, flops, nbytes, name):
    specs = [pl.BlockSpec(memory_space=pltpu.SMEM)] + vmem(len(args) - 1)
    return pl.pallas_call(
        kernel,
        out_shape=outs,
        in_specs=specs,
        out_specs=vmem(len(outs)),
        scratch_shapes=scratch,
        cost_estimate=pl.CostEstimate(flops=flops, bytes_accessed=nbytes, transcendentals=0),
        name=name,
    )(*args)


def struct(*shape, dtype=BF):
    return jax.ShapeDtypeStruct(shape, dtype)


def per_device(
    tokens, gain, w_ret_q, w_ret_k, w_ret_v, w_fox_q, w_fox_k, w_fox_v, fox_gates, w_out_ret, w_out_fox
):
    rates = jnp.asarray(RATE_ROWS)
    own = lax.all_to_all(jnp.broadcast_to(tokens[None], (4, 32, 2048)), "x", 0, 0, tiled=True)
    other = swapped(own)
    wt = jnp.concatenate([w_out_ret, w_out_fox], axis=0).reshape(3, LANES, 32).transpose(0, 2, 1)
    m1, states, kvg, qrot, inner = call(
        project_kernel,
        [struct(N, R1, LANES), struct(N, 64, LANES), struct(KG0 + 16, LANES), struct(RUN, RET), struct(RUN, RET, dtype=F32)],
        [pltpu.VMEM((RUN, 2048), BF)],
        (
            rates, own, other, gain.reshape(1, 2048), w_ret_q, w_ret_k, w_ret_v, w_fox_q, w_fox_k, w_fox_v,
            fox_gates.reshape(2, LANES), wt, jnp.asarray(ROW_TURN), jnp.asarray(RUN_TURN),
        ),
        1_400_000_000, 8_000_000, "project",
    )
    m1 = lax.dynamic_update_slice(m1, swapped(states), (0, SB0, 0))
    got1 = exchanged(m1, GROUPS_A)
    (m2,) = call(totals_kernel, [struct(N, R2, LANES)], [], (rates, got1, kvg), 1_000_000, 4_000_000, "totals")
    got2 = exchanged(m2, GROUPS_B)
    (m3,) = call(
        attention_kernel,
        [struct(N, R3, LANES)],
        [pltpu.VMEM((N, RUN, 2 * LANES), BF), pltpu.VMEM((N, RUN, 2 * LANES), BF)],
        (rates, got1, got2), 4_300_000_000, 4_000_000, "attention",
    )
    got3 = exchanged(m3, GROUPS_A)
    sent = swapped(got3[:, CB0 : CB0 + 64, :])
    keep, give = call(
        output_kernel,
        [struct(4, 32, 2048, dtype=F32), struct(4, 32, 2048)],
        [pltpu.VMEM((2048, 384), BF), pltpu.VMEM((RUN, 384), BF), pltpu.VMEM((RET, RET), BF)],
        (rates, got2, got3, sent, qrot, inner), 400_000_000, 4_000_000, "output",
    )
    pair = (keep + swapped(give).astype(F32)).astype(BF)
    return jnp.sum(lax.all_to_all(pair, "x", 0, 0, tiled=True).astype(F32), axis=0).astype(BF)


def solution(mesh):
    split = Mesh(mesh.devices.reshape(N, N, 4, 2), ALL)
    return jax.shard_map(
        per_device,
        mesh=split,
        in_specs=(
            P(ALL, None),
            P(),
            P(None, TP),
            P(None, TP),
            P(None, TP),
            P(None, TP),
            P(None, TP),
            P(None, TP),
            P(SP, TP),
            P(TP, SP),
            P(TP, SP),
        ),
        out_specs=P(ALL, None),
        check_vma=False,
    )
```

time: 494 us -> 168 us (0.34)
  the two profiles are of different devices: /device:TPU:496 before, /device:TPU:1 now
where the time goes in v1:
time: 168 us; the launch traced here: 167 us
  blocking collectives  112 us (67%)
  Pallas kernels  26.3 us (16%)
  starting transfers between devices  18.2 us (11%)
  waiting for transfers between devices  4.04 us (2%)
  other arithmetic  3.42 us (2%)
  local copies, waits for them, and re-layouts  3.08 us (2%)
    all_to_all x3, blocking collectives, exchanged(): lax.all_to_all(message, ALL, 0, 0, axis_index_groups=groups, tiled=True)  89 us
    pallas_call x4, Pallas kernels, call(): pl.pallas_call(kernel, out_shape=outs, in_specs=specs, out_specs=vmem(len...  26.3 us
    ppermute x4, starting transfers between devices, swapped(): return lax.ppermute(array, 'c', [(0, 1), (1, 0)])  18.2 us
    all_to_all x1, blocking collectives, per_device(): lax.all_to_all(pair, 'x', 0, 0, tiled=True).astype(F32)  11.6 us
    all_to_all x1, blocking collectives, per_device(): lax.all_to_all(jnp.broadcast_to(tokens[None], (4, 32, 2048)), 'x', 0, 0,...  11.6 us
    ppermute x4, waiting for transfers between devices, swapped(): return lax.ppermute(array, 'c', [(0, 1), (1, 0)])  4.04 us
  transfers between devices with their start and end apart: 4, of which 4 were waited for; matrix products, arithmetic and copies ran while one was open for 1% of the time, Pallas kernels for 0%

profile of v1, /device:TPU:1, one launch (start us, length us, event | category | flops | bytes accessed | tf_op | source)
XLA Modules:
  0.0 167.2 jit_solution(2869258952912948794)
XLA Ops:
  0.0 0.9 broadcast_in_dim.2
  1.0 11.6 %all_to_all.25.own = bf16[4,32,2048]{2,1,0:T(8,128)(2,1)S(1)} all-to-all(bf16[4,32,2048]{2,1,0:T(8,128)(2,1)S(1)} %broadcast_in_dim.2), channel_id=1, replica_groups=mesh['z'=8,'y'=8,'x'=4,'c'=2] {'x'}, dimensions={0} | all-to-all | bytes 1048576 | tf_op jit(solution)/shard_map/all_to_all | solution.py:278
  12.5 7.7 %collective-permute-start = (bf16[4,32,2048]{2,1,0:T(8,128)(2,1)S(1)}, bf16[4,32,2048]{2,1,0:T(8,128)(2,1)S(1)}, u32[]{:S(2)}, u32[]{:S(2)}) collective-permute-start(bf16[4,32,2048]{2,1,0:T(8,128)(2,1)S(1)} %all_to_all.25.own), channel_id=1, source_target_pairs={{0,1},{1,0},{2,3},{3,2},{4,5},{5,4},{6,7},{7,6},{8,9},{9,8},{10,11... | collective-permute-start | bytes 1572872 | tf_op jit(solution)/shard_map/ppermute | solution.py:55
  20.2 1.4 bitcast_bitcast_fusion.wt
  21.5 0.2 collective-permute-done.other
  21.7 0.8 copy-done.2
  22.5 6.7 %project.1 = (bf16[8,496,128]{2,1,0:T(8,128)(2,1)}, bf16[8,64,128]{2,1,0:T(8,128)(2,1)}, bf16[528,128]{1,0:T(8,128)(2,1)}, bf16[256,256]{1,0:T(8,128)(2,1)}, f32[256,256]{1,0:T(8,128)}) custom-call(f32[3,8]{1,0:T(4,128)} %constant.13.clone.rates, bf16[4,32,2048]{2,1,0:T(8,128)(2,1)} %copy-done.1, bf16[4,32,2048]{2,1,0:T(8,128)(2,1)} %copy-done.2, ...), custom_call_target="tpu_custom_call" | custom-call | flops 1400000000 | bytes 8000000 | tf_op jit(solution)/shard_map/project/pallas_call | solution.py:259
  29.2 2.3 %collective-permute-start.1 = (bf16[8,64,128]{2,1,0:T(8,128)(2,1)}, bf16[8,64,128]{2,1,0:T(8,128)(2,1)S(1)}, u32[]{:S(2)}, u32[]{:S(2)}) collective-permute-start(bf16[8,64,128]{2,1,0:T(8,128)(2,1)} %get-tuple-element.13), channel_id=1, source_target_pairs={{0,1},{1,0},{2,3},{3,2},{4,5},{5,4},{6,7},{7,6},{8,9},{9,8},{10,11... | collective-permute-start | bytes 393224 | tf_op jit(solution)/shard_map/ppermute | solution.py:55
  31.5 1.2 collective-permute-done.1
  32.6 0.7 constant_dynamic-update-slice_fusion
  33.3 25.3 %all_to_all.26.got1 = bf16[8,496,128]{2,1,0:T(8,128)(2,1)} all-to-all(bf16[8,496,128]{2,1,0:T(8,128)(2,1)} %constant_dynamic-update-slice_fusion), channel_id=1, replica_groups={{0,8,16,24,32,40,48,56},{2,10,18,26,34,42,50,58},{4,12,20,28,36,44,52,6..., dimensions={0} | all-to-all | bytes 2031616 | tf_op jit(solution)/shard_map/all_to_all | solution.py:51
  58.6 3.2 %totals.1 = bf16[8,1424,128]{2,1,0:T(8,128)(2,1)} custom-call(f32[3,8]{1,0:T(4,128)} %constant.13.clone.rates, bf16[8,496,128]{2,1,0:T(8,128)(2,1)} %all_to_all.26.got1, bf16[528,128]{1,0:T(8,128)(2,1)} %get-tuple-element.14.kvg), custom_call_target="tpu_custom_call" | custom-call | flops 1000000 | bytes 4000000 | tf_op jit(solution)/shard_map/totals/pallas_call | solution.py:259
  61.8 44.7 %all_to_all.27.got2 = bf16[8,1424,128]{2,1,0:T(8,128)(2,1)} all-to-all(bf16[8,1424,128]{2,1,0:T(8,128)(2,1)} %totals.1), channel_id=1, replica_groups={{0,64,128,192,256,320,384,448},{2,66,130,194,258,322,386,450},{4,68,132..., dimensions={0} | all-to-all | bytes 5832704 | tf_op jit(solution)/shard_map/all_to_all | solution.py:51
  106.5 11.8 %attention.1 = bf16[8,400,128]{2,1,0:T(8,128)(2,1)} custom-call(f32[3,8]{1,0:T(4,128)} %constant.13.clone.rates, bf16[8,496,128]{2,1,0:T(8,128)(2,1)} %all_to_all.26.got1, bf16[8,1424,128]{2,1,0:T(8,128)(2,1)} %all_to_all.27.got2), custom_call_target="tpu_custom_call" | custom-call | flops 4300000256 | bytes 4000000 | tf_op jit(solution)/shard_map/attention/pallas_call | solution.py:259
  118.3 19.0 %all_to_all.28.got3 = bf16[8,400,128]{2,1,0:T(8,128)(2,1)S(1)} all-to-all(bf16[8,400,128]{2,1,0:T(8,128)(2,1)} %attention.1), channel_id=1, replica_groups={{0,8,16,24,32,40,48,56},{2,10,18,26,34,42,50,58},{4,12,20,28,36,44,52,6..., dimensions={0} | all-to-all | bytes 1638400 | tf_op jit(solution)/shard_map/all_to_all | solution.py:51
  137.4 6.0 %collective-permute-start.2 = (bf16[8,64,128]{2,1,0:T(8,128)(2,1)S(1)}, bf16[8,64,128]{2,1,0:T(8,128)(2,1)S(1)}, u32[]{:S(2)}, u32[]{:S(2)}) collective-permute-start(bf16[8,64,128]{2,1,0:T(8,128)(2,1)S(1)} %slice.4), channel_id=1, source_target_pairs={{0,1},{1,0},{2,3},{3,2},{4,5},{5,4},{6,7},{7,6},{8,9},{9,8},{10,11... | collective-permute-start | bytes 393224 | tf_op jit(solution)/shard_map/ppermute | solution.py:55
  143.4 1.0 collective-permute-done.2.sent
  144.3 0.7 copy-done.3
  145.0 4.6 %output.1 = (f32[4,32,2048]{2,1,0:T(8,128)}, bf16[4,32,2048]{2,1,0:T(8,128)(2,1)}) custom-call(f32[3,8]{1,0:T(4,128)} %constant.13.clone.rates, bf16[8,1424,128]{2,1,0:T(8,128)(2,1)} %all_to_all.27.got2, bf16[8,400,128]{2,1,0:T(8,128)(2,1)} %copy-done, bf16[8,64,128]{2,1,0:T(8,128)(2,1)} %copy-done.3, bf16[256,256]{1,0:T(8,128)(2,1)} %get-tuple-element.15.qrot, ...), custom_call_target="tpu_custom_call" | custom-call | flops 400000000 | bytes 4000000 | tf_op jit(solution)/shard_map/output/pallas_call | solution.py:259
  149.6 2.3 %collective-permute-start.3 = (bf16[4,32,2048]{2,1,0:T(8,128)(2,1)}, bf16[4,32,2048]{2,1,0:T(8,128)(2,1)S(1)}, u32[]{:S(2)}, u32[]{:S(2)}) collective-permute-start(bf16[4,32,2048]{2,1,0:T(8,128)(2,1)} %get-tuple-element.18), channel_id=1, source_target_pairs={{0,1},{1,0},{2,3},{3,2},{4,5},{5,4},{6,7},{7,6},{8,9},{9,8},{10,11... | collective-permute-start | bytes 1572872 | tf_op jit(solution)/shard_map/ppermute | solution.py:55
  151.8 1.7 %collective-permute-done.3 = bf16[4,32,2048]{2,1,0:T(8,128)(2,1)S(1)} collective-permute-done((bf16[4,32,2048]{2,1,0:T(8,128)(2,1)}, bf16[4,32,2048]{2,1,0:T(8,128)(2,1)S(1)}, u32[]{:S(2)}, u32[]{:S(2)}) %collective-permute-start.3) | collective-permute-done | bytes 524320 | tf_op jit(solution)/shard_map/ppermute | solution.py:55
  153.6 1.3 add_convert_fusion
  154.9 11.6 %all_to_all.29 = bf16[4,32,2048]{2,1,0:T(8,128)(2,1)S(1)} all-to-all(bf16[4,32,2048]{2,1,0:T(8,128)(2,1)S(1)} %add_convert_fusion), channel_id=1, replica_groups=mesh['z'=8,'y'=8,'x'=4,'c'=2] {'x'}, dimensions={0} | all-to-all | bytes 1048576 | tf_op jit(solution)/shard_map/all_to_all | solution.py:310
  166.5 0.7 reduce_sum.12
  (7 shorter events, 0.0 us)
Async XLA Ops:
  12.5 9.2 %copy-start.1 = (bf16[4,32,2048]{2,1,0:T(8,128)(2,1)}, bf16[4,32,2048]{2,1,0:T(8,128)(2,1)S(1)}, u32[]{:S(2)}) copy-start(bf16[4,32,2048]{2,1,0:T(8,128)(2,1)S(1)} %all_to_all.25.own) | copy-start | bytes 1572868
  12.5 9.2 %collective-permute-start = (bf16[4,32,2048]{2,1,0:T(8,128)(2,1)S(1)}, bf16[4,32,2048]{2,1,0:T(8,128)(2,1)S(1)}, u32[]{:S(2)}, u32[]{:S(2)}) collective-permute-start(bf16[4,32,2048]{2,1,0:T(8,128)(2,1)S(1)} %all_to_all.25.own), channel_id=1, source_target_pairs={{0,1},{1,0},{2,3},{3,2},{4,5},{5,4},{6,7},{7,6},{8,9},{9,8},{10,11... | collective-permute-start | bytes 1572872 | tf_op jit(solution)/shard_map/ppermute | solution.py:55
  21.7 0.8 copy-start.2
  29.2 3.5 %collective-permute-start.1 = (bf16[8,64,128]{2,1,0:T(8,128)(2,1)}, bf16[8,64,128]{2,1,0:T(8,128)(2,1)S(1)}, u32[]{:S(2)}, u32[]{:S(2)}) collective-permute-start(bf16[8,64,128]{2,1,0:T(8,128)(2,1)} %get-tuple-element.13), channel_id=1, source_target_pairs={{0,1},{1,0},{2,3},{3,2},{4,5},{5,4},{6,7},{7,6},{8,9},{9,8},{10,11... | collective-permute-start | bytes 393224 | tf_op jit(solution)/shard_map/ppermute | solution.py:55
  137.4 7.0 %copy-start = (bf16[8,400,128]{2,1,0:T(8,128)(2,1)}, bf16[8,400,128]{2,1,0:T(8,128)(2,1)S(1)}, u32[]{:S(2)}) copy-start(bf16[8,400,128]{2,1,0:T(8,128)(2,1)S(1)} %all_to_all.28.got3) | copy-start | bytes 2457604
  137.4 6.9 %collective-permute-start.2 = (bf16[8,64,128]{2,1,0:T(8,128)(2,1)S(1)}, bf16[8,64,128]{2,1,0:T(8,128)(2,1)S(1)}, u32[]{:S(2)}, u32[]{:S(2)}) collective-permute-start(bf16[8,64,128]{2,1,0:T(8,128)(2,1)S(1)} %slice.4), channel_id=1, source_target_pairs={{0,1},{1,0},{2,3},{3,2},{4,5},{5,4},{6,7},{7,6},{8,9},{9,8},{10,11... | collective-permute-start | bytes 393224 | tf_op jit(solution)/shard_map/ppermute | solution.py:55
  144.3 0.7 copy-start.3
  149.6 4.0 %collective-permute-start.3 = (bf16[4,32,2048]{2,1,0:T(8,128)(2,1)}, bf16[4,32,2048]{2,1,0:T(8,128)(2,1)S(1)}, u32[]{:S(2)}, u32[]{:S(2)}) collective-permute-start(bf16[4,32,2048]{2,1,0:T(8,128)(2,1)} %get-tuple-element.18), channel_id=1, source_target_pairs={{0,1},{1,0},{2,3},{3,2},{4,5},{5,4},{6,7},{7,6},{8,9},{9,8},{10,11... | collective-permute-start | bytes 1572872 | tf_op jit(solution)/shard_map/ppermute | solution.py:55

commit v2 on v1

--- a/solution.py
+++ b/solution.py
@@ -26,7 +26,8 @@
 
 HEADS = np.arange(8, dtype=np.float64)
 RATES = np.where(HEADS < 4, 1.0 / (32.0 + 16.0 * HEADS), np.exp2(-(HEADS - 4)) / 16384.0)
-RATE_ROWS = np.stack([RATES, np.exp(-RATES * RUN), np.exp(-RATES * RUN * N)]).astype(np.float32)
+PER_RUN = np.exp(-RATES * RUN)
+PER_ROW = np.exp(-RATES * RUN * N)
 INVERSE = 10000.0 ** (-np.arange(LANES, dtype=np.float64) / LANES)
 ROW_ANGLE = np.arange(RUN, dtype=np.float64)[:, None] * INVERSE
 RUN_ANGLE = (RUN * np.arange(64, dtype=np.float64))[:, None] * INVERSE
@@ -61,6 +62,13 @@
     return z * N + y, jnp.where(first, y, z), jnp.where(first, z, y), c
 
 
+def of_head(table, head):
+    value = jnp.float32(table[0])
+    for h in range(1, 8):
+        value = jnp.where(head == h, jnp.float32(table[h]), value)
+    return value
+
+
 def dot_nt(left, right):
     return lax.dot_general(left, right, (((1,), (1,)), ((), ())), preferred_element_type=F32)
 
@@ -73,19 +81,27 @@
     return jnp.dot(left, right, preferred_element_type=F32)
 
 
-def project_kernel(
-    rates, own, other, gain, wrq, wrk, wrv, wfq, wfk, wfv, gates, wt, row_turn, run_turn,
-    m1, states, kvg, qrot, inner, xs,
-):
+def project_kernel(*refs):
+    own, other, wt = refs[:3]
+    far = refs[3:13]
+    m1, states, kvg, qrot, inner, xs = refs[13:19]
+    near = refs[19:29]
+    sems = refs[29]
+    copies = [pltpu.make_async_copy(src, dst, sems.at[k]) for k, (src, dst) in enumerate(zip(far, near))]
+    for copy in copies:
+        copy.start()
+    gain, wrk, wrv, row_turn, run_turn, wrq, wfq, wfk, wfv, gates = near
     place, _, _, c = places()
-    head = lax.axis_index("x") * 2 + c
-    rate = rates[0, head]
+    rate = of_head(RATES, lax.axis_index("x") * 2 + c)
+    copies[0].wait()
     for j in range(4):
         for part, side in ((own, c), (other, 1 - c)):
             x = part[j].astype(F32)
             scaled = x * lax.rsqrt(jnp.mean(x * x, axis=1, keepdims=True) + eps) * gain[...]
             xs[pl.ds(pl.multiple_of(64 * j + 32 * side, 32), 32), :] = scaled.astype(BF)
     x = xs[...]
+    for copy in copies[1:5]:
+        copy.wait()
     cos_run = run_turn[0, pl.ds(place, 1), :]
     sin_run = run_turn[1, pl.ds(place, 1), :]
     cosine = row_turn[0] * cos_run - row_turn[1] * sin_run
@@ -109,6 +125,8 @@
             states[j, 32 * half : 32 * half + 32, :] = piece
             m1[j, SA0 + 32 * half : SA0 + 32 * half + 32, :] = piece
             m1[j, SB0 + 32 * half : SB0 + 32 * half + 32, :] = piece
+    for copy in copies[5:]:
+        copy.wait()
     rq = turned(dot(x, wrq[...]).astype(BF).astype(F32), 1.0).astype(BF)
     qrot[...] = rq
     spread = row - col
@@ -135,11 +153,11 @@
             m1[j, W0 + 32 * k : W0 + 32 * k + 32, :] = wt[k]
 
 
-def totals_kernel(rates, got1, kvg, m2):
+def totals_kernel(got1, kvg, m2):
     head = lax.axis_index("x") * 2 + lax.axis_index("c")
     sums = []
     for start, which in ((SA0, head), (SB0, head ^ 1)):
-        decay = rates[1, which]
+        decay = of_head(PER_RUN, which)
         total = got1[0, start : start + 64, :].astype(F32)
         for j in range(1, N):
             total = total * decay + got1[j, start : start + 64, :].astype(F32)
@@ -159,7 +177,7 @@
     return dot_nt(eye, wide).astype(BF)
 
 
-def attention_kernel(rates, got1, got2, m3, keys, values):
+def attention_kernel(got1, got2, m3, keys, values):
     _, a, b, c = places()
     head = lax.axis_index("x") * 2 + c
     row = lax.broadcasted_iota(jnp.int32, (RUN, RUN), 0)
@@ -198,7 +216,7 @@
     lax.fori_loop(0, N, one_run, 0)
     for own, (sums, slices, carried) in enumerate(((TA0, SA0, CA0), (TB0, SB0, CB0))):
         which = head ^ own
-        per_run, per_row = rates[1, which], rates[2, which]
+        per_run, per_row = of_head(PER_RUN, which), of_head(PER_ROW, which)
         state = jnp.zeros((64, LANES), F32)
         for k in range(N):
             state = jnp.where(k < b, state * per_row + got2[k, sums : sums + 64, :].astype(F32), state)
@@ -207,9 +225,9 @@
             state = state * per_run + got1[j, slices : slices + 64, :].astype(F32)
 
 
-def output_kernel(rates, got2, got3, sent, qrot, inner, keep, give, weight, mixed, state):
+def output_kernel(got2, got3, sent, qrot, inner, keep, give, weight, mixed, state):
     _, _, _, c = places()
-    rate = rates[0, lax.axis_index("x") * 2 + c]
+    rate = of_head(RATES, lax.axis_index("x") * 2 + c)
     for i in range(N):
         for k in range(N):
             at = pl.multiple_of(jnp.where(c == 0, i * N + k, k * N + i) * 32, 32)
@@ -254,8 +272,8 @@
     return [pl.BlockSpec(memory_space=pltpu.VMEM)] * count
 
 
-def call(kernel, outs, scratch, args, flops, nbytes, name):
-    specs = [pl.BlockSpec(memory_space=pltpu.SMEM)] + vmem(len(args) - 1)
+def call(kernel, outs, scratch, args, flops, nbytes, name, limit, far=()):
+    specs = vmem(len(args)) + [pl.BlockSpec(memory_space=pltpu.HBM)] * len(far)
     return pl.pallas_call(
         kernel,
         out_shape=outs,
@@ -263,8 +281,9 @@
         out_specs=vmem(len(outs)),
         scratch_shapes=scratch,
         cost_estimate=pl.CostEstimate(flops=flops, bytes_accessed=nbytes, transcendentals=0),
+        compiler_params=pltpu.CompilerParams(vmem_limit_bytes=limit << 20),
         name=name,
-    )(*args)
+    )(*args, *far)
 
 
 def struct(*shape, dtype=BF):
@@ -274,29 +293,28 @@
 def per_device(
     tokens, gain, w_ret_q, w_ret_k, w_ret_v, w_fox_q, w_fox_k, w_fox_v, fox_gates, w_out_ret, w_out_fox
 ):
-    rates = jnp.asarray(RATE_ROWS)
     own = lax.all_to_all(jnp.broadcast_to(tokens[None], (4, 32, 2048)), "x", 0, 0, tiled=True)
     other = swapped(own)
     wt = jnp.concatenate([w_out_ret, w_out_fox], axis=0).reshape(3, LANES, 32).transpose(0, 2, 1)
+    far = (
+        gain.reshape(1, 2048), w_ret_k, w_ret_v, jnp.asarray(ROW_TURN), jnp.asarray(RUN_TURN),
+        w_ret_q, w_fox_q, w_fox_k, w_fox_v, fox_gates.reshape(2, LANES),
+    )
     m1, states, kvg, qrot, inner = call(
         project_kernel,
         [struct(N, R1, LANES), struct(N, 64, LANES), struct(KG0 + 16, LANES), struct(RUN, RET), struct(RUN, RET, dtype=F32)],
-        [pltpu.VMEM((RUN, 2048), BF)],
-        (
-            rates, own, other, gain.reshape(1, 2048), w_ret_q, w_ret_k, w_ret_v, w_fox_q, w_fox_k, w_fox_v,
-            fox_gates.reshape(2, LANES), wt, jnp.asarray(ROW_TURN), jnp.asarray(RUN_TURN),
-        ),
-        1_400_000_000, 8_000_000, "project",
+        [pltpu.VMEM((RUN, 2048), BF)] + [pltpu.VMEM(a.shape, a.dtype) for a in far] + [pltpu.SemaphoreType.DMA((len(far),))],
+        (own, other, wt), 1_400_000_000, 8_000_000, "project", 60, far,
     )
     m1 = lax.dynamic_update_slice(m1, swapped(states), (0, SB0, 0))
     got1 = exchanged(m1, GROUPS_A)
-    (m2,) = call(totals_kernel, [struct(N, R2, LANES)], [], (rates, got1, kvg), 1_000_000, 4_000_000, "totals")
+    (m2,) = call(totals_kernel, [struct(N, R2, LANES)], [], (got1, kvg), 1_000_000, 4_000_000, "totals", 16)
     got2 = exchanged(m2, GROUPS_B)
     (m3,) = call(
         attention_kernel,
         [struct(N, R3, LANES)],
         [pltpu.VMEM((N, RUN, 2 * LANES), BF), pltpu.VMEM((N, RUN, 2 * LANES), BF)],
-        (rates, got1, got2), 4_300_000_000, 4_000_000, "attention",
+        (got1, got2), 4_300_000_000, 4_000_000, "attention", 24,
     )
     got3 = exchanged(m3, GROUPS_A)
     sent = swapped(got3[:, CB0 : CB0 + 64, :])
@@ -304,7 +322,7 @@
         output_kernel,
         [struct(4, 32, 2048, dtype=F32), struct(4, 32, 2048)],
         [pltpu.VMEM((2048, 384), BF), pltpu.VMEM((RUN, 384), BF), pltpu.VMEM((RET, RET), BF)],
-        (rates, got2, got3, sent, qrot, inner), 400_000_000, 4_000_000, "output",
+        (got2, got3, sent, qrot, inner), 400_000_000, 4_000_000, "output", 20,
     )
     pair = (keep + swapped(give).astype(F32)).astype(BF)
     return jnp.sum(lax.all_to_all(pair, "x", 0, 0, tiled=True).astype(F32), axis=0).astype(BF)

time: 168 us -> 157 us (0.935)
  Pallas kernels: 26.3 us -> 17.6 us
    pallas_call x4, Pallas kernels: 26.3 us -> 17.6 us  [call(): pl.pallas_call(kernel, out_shape=outs, in_specs=specs, out_specs=vmem(len...]
where the time goes in v2:
time: 157 us; the launch traced here: 156 us
  blocking collectives  111 us (71%)
  starting transfers between devices  18.2 us (12%)
  Pallas kernels  17.6 us (11%)
  waiting for transfers between devices  3.86 us (2%)
  local copies, waits for them, and re-layouts  3.37 us (2%)
  other arithmetic  2.19 us (1%)
    all_to_all x3, blocking collectives, exchanged(): lax.all_to_all(message, ALL, 0, 0, axis_index_groups=groups, tiled=True)  87.6 us
    ppermute x4, starting transfers between devices, swapped(): return lax.ppermute(array, 'c', [(0, 1), (1, 0)])  18.2 us
    pallas_call x4, Pallas kernels, call(): pl.pallas_call(kernel, out_shape=outs, in_specs=specs, out_specs=vmem(len...  17.6 us
    all_to_all x1, blocking collectives, per_device(): lax.all_to_all(pair, 'x', 0, 0, tiled=True).astype(F32)  11.6 us
    all_to_all x1, blocking collectives, per_device(): lax.all_to_all(jnp.broadcast_to(tokens[None], (4, 32, 2048)), 'x', 0, 0,...  11.6 us
    ppermute x4, waiting for transfers between devices, swapped(): return lax.ppermute(array, 'c', [(0, 1), (1, 0)])  3.86 us
  transfers between devices with their start and end apart: 4, of which 4 were waited for; matrix products, arithmetic and copies ran while one was open for 1% of the time, Pallas kernels for 0%

profile of v2, /device:TPU:1, one launch (start us, length us, event | category | flops | bytes accessed | tf_op | source)
XLA Modules:
  0.0 156.0 jit_solution(4956270813591635194)
XLA Ops:
  0.0 0.9 broadcast_in_dim.2
  1.0 11.6 %all_to_all.25.refs_0_ = bf16[4,32,2048]{2,1,0:T(8,128)(2,1)S(1)} all-to-all(bf16[4,32,2048]{2,1,0:T(8,128)(2,1)S(1)} %broadcast_in_dim.2), channel_id=1, replica_groups=mesh['z'=8,'y'=8,'x'=4,'c'=2] {'x'}, dimensions={0} | all-to-all | bytes 1048576 | tf_op jit(solution)/shard_map/all_to_all | solution.py:296
  12.5 7.7 %collective-permute-start = (bf16[4,32,2048]{2,1,0:T(8,128)(2,1)S(1)}, bf16[4,32,2048]{2,1,0:T(8,128)(2,1)S(1)}, u32[]{:S(2)}, u32[]{:S(2)}) collective-permute-start(bf16[4,32,2048]{2,1,0:T(8,128)(2,1)S(1)} %all_to_all.25.refs_0_), channel_id=1, source_target_pairs={{0,1},{1,0},{2,3},{3,2},{4,5},{5,4},{6,7},{7,6},{8,9},{9,8},{10,11... | collective-permute-start | bytes 1572872 | tf_op jit(solution)/shard_map/ppermute | solution.py:56
  20.2 1.3 bitcast_bitcast_fusion.refs_2_
  21.5 0.2 collective-permute-done.refs_1_
  21.7 0.8 copy-done.4
  22.5 6.8 %project.1 = (bf16[8,496,128]{2,1,0:T(8,128)(2,1)}, bf16[8,64,128]{2,1,0:T(8,128)(2,1)}, bf16[528,128]{1,0:T(8,128)(2,1)}, bf16[256,256]{1,0:T(8,128)(2,1)}, f32[256,256]{1,0:T(8,128)}) custom-call(bf16[4,32,2048]{2,1,0:T(8,128)(2,1)} %copy-done.3, bf16[4,32,2048]{2,1,0:T(8,128)(2,1)} %copy-done.4, bf16[3,32,128]{2,1,0:T(8,128)(2,1)} %bitcast_bitcast_fusion.refs_2_, ...), custom_call_target="tpu_custom_call" | custom-call | flops 1400000000 | bytes 8000000 | tf_op jit(solution)/shard_map/project/pallas_call | solution.py:277
  29.3 2.3 %collective-permute-start.1 = (bf16[8,64,128]{2,1,0:T(8,128)(2,1)}, bf16[8,64,128]{2,1,0:T(8,128)(2,1)S(1)}, u32[]{:S(2)}, u32[]{:S(2)}) collective-permute-start(bf16[8,64,128]{2,1,0:T(8,128)(2,1)} %get-tuple-element.13), channel_id=1, source_target_pairs={{0,1},{1,0},{2,3},{3,2},{4,5},{5,4},{6,7},{7,6},{8,9},{9,8},{10,11... | collective-permute-start | bytes 393224 | tf_op jit(solution)/shard_map/ppermute | solution.py:56
  31.6 1.2 collective-permute-done.1
  32.7 0.7 constant_dynamic-update-slice_fusion
  33.4 25.2 %all_to_all.26.got1 = bf16[8,496,128]{2,1,0:T(8,128)(2,1)S(1)} all-to-all(bf16[8,496,128]{2,1,0:T(8,128)(2,1)} %constant_dynamic-update-slice_fusion), channel_id=1, replica_groups={{0,8,16,24,32,40,48,56},{2,10,18,26,34,42,50,58},{4,12,20,28,36,44,52,6..., dimensions={0} | all-to-all | bytes 2031616 | tf_op jit(solution)/shard_map/all_to_all | solution.py:52
  58.6 0.9 copy-done.1
  59.5 0.4 totals.1
  59.9 44.4 %all_to_all.27.got2 = bf16[8,1424,128]{2,1,0:T(8,128)(2,1)S(1)} all-to-all(bf16[8,1424,128]{2,1,0:T(8,128)(2,1)S(1)} %totals.1), channel_id=1, replica_groups={{0,64,128,192,256,320,384,448},{2,66,130,194,258,322,386,450},{4,68,132..., dimensions={0} | all-to-all | bytes 5832704 | tf_op jit(solution)/shard_map/all_to_all | solution.py:52
  104.3 8.8 %attention.1 = bf16[8,400,128]{2,1,0:T(8,128)(2,1)S(1)} custom-call(bf16[8,496,128]{2,1,0:T(8,128)(2,1)S(1)} %all_to_all.26.got1, bf16[8,1424,128]{2,1,0:T(8,128)(2,1)S(1)} %all_to_all.27.got2), custom_call_target="tpu_custom_call" | custom-call | flops 4300000256 | bytes 4000000 | tf_op jit(solution)/shard_map/attention/pallas_call | solution.py:277
  113.1 18.0 %all_to_all.28.got3 = bf16[8,400,128]{2,1,0:T(8,128)(2,1)S(1)} all-to-all(bf16[8,400,128]{2,1,0:T(8,128)(2,1)S(1)} %attention.1), channel_id=1, replica_groups={{0,8,16,24,32,40,48,56},{2,10,18,26,34,42,50,58},{4,12,20,28,36,44,52,6..., dimensions={0} | all-to-all | bytes 1638400 | tf_op jit(solution)/shard_map/all_to_all | solution.py:52
  131.1 6.0 %collective-permute-start.2 = (bf16[8,64,128]{2,1,0:T(8,128)(2,1)S(1)}, bf16[8,64,128]{2,1,0:T(8,128)(2,1)S(1)}, u32[]{:S(2)}, u32[]{:S(2)}) collective-permute-start(bf16[8,64,128]{2,1,0:T(8,128)(2,1)S(1)} %slice.4), channel_id=1, source_target_pairs={{0,1},{1,0},{2,3},{3,2},{4,5},{5,4},{6,7},{7,6},{8,9},{9,8},{10,11... | collective-permute-start | bytes 393224 | tf_op jit(solution)/shard_map/ppermute | solution.py:56
  137.1 1.0 collective-permute-done.2.sent
  138.1 1.6 %output.1 = (f32[4,32,2048]{2,1,0:T(8,128)S(1)}, bf16[4,32,2048]{2,1,0:T(8,128)(2,1)S(1)}) custom-call(bf16[8,1424,128]{2,1,0:T(8,128)(2,1)S(1)} %all_to_all.27.got2, bf16[8,400,128]{2,1,0:T(8,128)(2,1)S(1)} %all_to_all.28.got3, bf16[8,64,128]{2,1,0:T(8,128)(2,1)S(1)} %collective-permute-done.2.sent, bf16[256,256]{1,0:T(8,128)(2,1)S(1)} %copy-done.2, ...), custom_call_target="tpu_custom_call" | custom-call | flops 400000000 | bytes 4000000 | tf_op jit(solution)/shard_map/output/pallas_call | solution.py:277
  139.7 2.2 %collective-permute-start.3 = (bf16[4,32,2048]{2,1,0:T(8,128)(2,1)S(1)}, bf16[4,32,2048]{2,1,0:T(8,128)(2,1)S(1)}, u32[]{:S(2)}, u32[]{:S(2)}) collective-permute-start(bf16[4,32,2048]{2,1,0:T(8,128)(2,1)S(1)} %get-tuple-element.18), channel_id=1, source_target_pairs={{0,1},{1,0},{2,3},{3,2},{4,5},{5,4},{6,7},{7,6},{8,9},{9,8},{10,11... | collective-permute-start | bytes 1572872 | tf_op jit(solution)/shard_map/ppermute | solution.py:56
  141.9 1.6 collective-permute-done.3
  143.5 0.1 add_convert_fusion
  143.6 11.6 %all_to_all.29 = bf16[4,32,2048]{2,1,0:T(8,128)(2,1)S(1)} all-to-all(bf16[4,32,2048]{2,1,0:T(8,128)(2,1)S(1)} %add_convert_fusion), channel_id=1, replica_groups=mesh['z'=8,'y'=8,'x'=4,'c'=2] {'x'}, dimensions={0} | all-to-all | bytes 1048576 | tf_op jit(solution)/shard_map/all_to_all | solution.py:328
  155.2 0.7 reduce_sum.12
  (9 shorter events, 0.0 us)
Async XLA Ops:
  12.5 9.2 %copy-start.3 = (bf16[4,32,2048]{2,1,0:T(8,128)(2,1)}, bf16[4,32,2048]{2,1,0:T(8,128)(2,1)S(1)}, u32[]{:S(2)}) copy-start(bf16[4,32,2048]{2,1,0:T(8,128)(2,1)S(1)} %all_to_all.25.refs_0_) | copy-start | bytes 1572868
  12.5 9.2 %collective-permute-start = (bf16[4,32,2048]{2,1,0:T(8,128)(2,1)S(1)}, bf16[4,32,2048]{2,1,0:T(8,128)(2,1)S(1)}, u32[]{:S(2)}, u32[]{:S(2)}) collective-permute-start(bf16[4,32,2048]{2,1,0:T(8,128)(2,1)S(1)} %all_to_all.25.refs_0_), channel_id=1, source_target_pairs={{0,1},{1,0},{2,3},{3,2},{4,5},{5,4},{6,7},{7,6},{8,9},{9,8},{10,11... | collective-permute-start | bytes 1572872 | tf_op jit(solution)/shard_map/ppermute | solution.py:56
  21.7 0.8 copy-start.4
  29.3 3.5 %collective-permute-start.1 = (bf16[8,64,128]{2,1,0:T(8,128)(2,1)}, bf16[8,64,128]{2,1,0:T(8,128)(2,1)S(1)}, u32[]{:S(2)}, u32[]{:S(2)}) collective-permute-start(bf16[8,64,128]{2,1,0:T(8,128)(2,1)} %get-tuple-element.13), channel_id=1, source_target_pairs={{0,1},{1,0},{2,3},{3,2},{4,5},{5,4},{6,7},{7,6},{8,9},{9,8},{10,11... | collective-permute-start | bytes 393224 | tf_op jit(solution)/shard_map/ppermute | solution.py:56
  58.6 0.9 copy-start.1
  104.3 33.8 %copy-start = (f32[256,256]{1,0:T(8,128)S(1)}, f32[256,256]{1,0:T(8,128)}, u32[]{:S(2)}) copy-start(f32[256,256]{1,0:T(8,128)} %get-tuple-element.16.inner) | copy-start | bytes 786436
  104.3 33.8 %copy-start.2 = (bf16[256,256]{1,0:T(8,128)(2,1)S(1)}, bf16[256,256]{1,0:T(8,128)(2,1)}, u32[]{:S(2)}) copy-start(bf16[256,256]{1,0:T(8,128)(2,1)} %get-tuple-element.15.qrot) | copy-start | bytes 393220
  131.1 6.9 %collective-permute-start.2 = (bf16[8,64,128]{2,1,0:T(8,128)(2,1)S(1)}, bf16[8,64,128]{2,1,0:T(8,128)(2,1)S(1)}, u32[]{:S(2)}, u32[]{:S(2)}) collective-permute-start(bf16[8,64,128]{2,1,0:T(8,128)(2,1)S(1)} %slice.4), channel_id=1, source_target_pairs={{0,1},{1,0},{2,3},{3,2},{4,5},{5,4},{6,7},{7,6},{8,9},{9,8},{10,11... | collective-permute-start | bytes 393224 | tf_op jit(solution)/shard_map/ppermute | solution.py:56
  139.7 3.8 %collective-permute-start.3 = (bf16[4,32,2048]{2,1,0:T(8,128)(2,1)S(1)}, bf16[4,32,2048]{2,1,0:T(8,128)(2,1)S(1)}, u32[]{:S(2)}, u32[]{:S(2)}) collective-permute-start(bf16[4,32,2048]{2,1,0:T(8,128)(2,1)S(1)} %get-tuple-element.18), channel_id=1, source_target_pairs={{0,1},{1,0},{2,3},{3,2},{4,5},{5,4},{6,7},{7,6},{8,9},{9,8},{10,11... | collective-permute-start | bytes 1572872 | tf_op jit(solution)/shard_map/ppermute | solution.py:56

commit v3 on v2

--- a/solution.py
+++ b/solution.py
@@ -196,12 +196,13 @@
             [got1[j, Q0 : Q0 + RUN, :], as_columns(got1[j, QG0 : QG0 + 16, :], eye)], axis=1
         )
         of_query = jnp.where(c == 0, b * N + j, j * N + b)
-        total = jnp.zeros((RUN, 2 * LANES), F32)
+        weights = []
         for i in range(N):
             of_key = jnp.where(c == 0, i * N + a, a * N + i)
             score = dot_nt(query, keys[i]) * (FOX**-0.5 * math.log2(math.e))
             score = jnp.where(ahead <= (of_query - of_key) * RUN, score, -jnp.inf)
-            total = total + dot(jnp.exp2(score).astype(BF), values[i])
+            weights.append(jnp.exp2(score).astype(BF))
+        total = dot(jnp.concatenate(weights, axis=1), values[...].reshape(N * RUN, 2 * LANES))
         m3[j, N0 : N0 + RUN, :] = total[:, :LANES].astype(BF)
         den = [
             jnp.sum(jnp.where(diagonal, total[LANES * h : LANES * h + LANES, LANES:], 0.0), axis=0, keepdims=True)
@@ -213,7 +214,7 @@
         m3[j, D0 : D0 + 16, :] = jnp.where(line < 2, high, jnp.where(line < 4, den - high, 0.0)).astype(BF)
         return carry
 
-    lax.fori_loop(0, N, one_run, 0)
+    lax.fori_loop(0, N, one_run, 0, unroll=4)
     for own, (sums, slices, carried) in enumerate(((TA0, SA0, CA0), (TB0, SB0, CB0))):
         which = head ^ own
         per_run, per_row = of_head(PER_RUN, which), of_head(PER_ROW, which)

time: 157 us -> 154 us (0.981)
  Pallas kernels: 17.6 us -> 15.2 us
    pallas_call x4, Pallas kernels: 17.6 us -> 15.2 us  [call(): pl.pallas_call(kernel, out_shape=outs, in_specs=specs, out_specs=vmem(len...]
where the time goes in v3:
time: 154 us
  blocking collectives  111 us (72%)
  starting transfers between devices  18.2 us (12%)
  Pallas kernels  15.2 us (10%)
  waiting for transfers between devices  3.83 us (2%)
  local copies, waits for them, and re-layouts  3.37 us (2%)
  other arithmetic  2.19 us (1%)
    all_to_all x3, blocking collectives, exchanged(): lax.all_to_all(message, ALL, 0, 0, axis_index_groups=groups, tiled=True)  87.6 us
    ppermute x4, starting transfers between devices, swapped(): return lax.ppermute(array, 'c', [(0, 1), (1, 0)])  18.2 us
    pallas_call x4, Pallas kernels, call(): pl.pallas_call(kernel, out_shape=outs, in_specs=specs, out_specs=vmem(len...  15.2 us
    all_to_all x1, blocking collectives, per_device(): lax.all_to_all(pair, 'x', 0, 0, tiled=True).astype(F32)  11.6 us
    all_to_all x1, blocking collectives, per_device(): lax.all_to_all(jnp.broadcast_to(tokens[None], (4, 32, 2048)), 'x', 0, 0,...  11.6 us
    ppermute x4, waiting for transfers between devices, swapped(): return lax.ppermute(array, 'c', [(0, 1), (1, 0)])  3.83 us
  transfers between devices with their start and end apart: 4, of which 4 were waited for; matrix products, arithmetic and copies ran while one was open for 1% of the time, Pallas kernels for 0%

profile of v3, /device:TPU:1, one launch (start us, length us, event | category | flops | bytes accessed | tf_op | source)
XLA Modules:
  0.0 153.6 jit_solution(17573742570661652664)
XLA Ops:
  0.0 0.9 broadcast_in_dim.2
  1.0 11.6 %all_to_all.25.refs_0_ = bf16[4,32,2048]{2,1,0:T(8,128)(2,1)S(1)} all-to-all(bf16[4,32,2048]{2,1,0:T(8,128)(2,1)S(1)} %broadcast_in_dim.2), channel_id=1, replica_groups=mesh['z'=8,'y'=8,'x'=4,'c'=2] {'x'}, dimensions={0} | all-to-all | bytes 1048576 | tf_op jit(solution)/shard_map/all_to_all | solution.py:297
  12.5 7.7 %collective-permute-start = (bf16[4,32,2048]{2,1,0:T(8,128)(2,1)S(1)}, bf16[4,32,2048]{2,1,0:T(8,128)(2,1)S(1)}, u32[]{:S(2)}, u32[]{:S(2)}) collective-permute-start(bf16[4,32,2048]{2,1,0:T(8,128)(2,1)S(1)} %all_to_all.25.refs_0_), channel_id=1, source_target_pairs={{0,1},{1,0},{2,3},{3,2},{4,5},{5,4},{6,7},{7,6},{8,9},{9,8},{10,11... | collective-permute-start | bytes 1572872 | tf_op jit(solution)/shard_map/ppermute | solution.py:56
  20.2 1.3 bitcast_bitcast_fusion.refs_2_
  21.5 0.2 collective-permute-done.refs_1_
  21.7 0.8 copy-done.4
  22.5 6.8 %project.1 = (bf16[8,496,128]{2,1,0:T(8,128)(2,1)}, bf16[8,64,128]{2,1,0:T(8,128)(2,1)}, bf16[528,128]{1,0:T(8,128)(2,1)}, bf16[256,256]{1,0:T(8,128)(2,1)}, f32[256,256]{1,0:T(8,128)}) custom-call(bf16[4,32,2048]{2,1,0:T(8,128)(2,1)} %copy-done.3, bf16[4,32,2048]{2,1,0:T(8,128)(2,1)} %copy-done.4, bf16[3,32,128]{2,1,0:T(8,128)(2,1)} %bitcast_bitcast_fusion.refs_2_, ...), custom_call_target="tpu_custom_call" | custom-call | flops 1400000000 | bytes 8000000 | tf_op jit(solution)/shard_map/project/pallas_call | solution.py:278
  29.3 2.3 %collective-permute-start.1 = (bf16[8,64,128]{2,1,0:T(8,128)(2,1)}, bf16[8,64,128]{2,1,0:T(8,128)(2,1)S(1)}, u32[]{:S(2)}, u32[]{:S(2)}) collective-permute-start(bf16[8,64,128]{2,1,0:T(8,128)(2,1)} %get-tuple-element.13), channel_id=1, source_target_pairs={{0,1},{1,0},{2,3},{3,2},{4,5},{5,4},{6,7},{7,6},{8,9},{9,8},{10,11... | collective-permute-start | bytes 393224 | tf_op jit(solution)/shard_map/ppermute | solution.py:56
  31.6 1.2 collective-permute-done.1
  32.7 0.7 constant_dynamic-update-slice_fusion
  33.4 25.2 %all_to_all.26.got1 = bf16[8,496,128]{2,1,0:T(8,128)(2,1)S(1)} all-to-all(bf16[8,496,128]{2,1,0:T(8,128)(2,1)} %constant_dynamic-update-slice_fusion), channel_id=1, replica_groups={{0,8,16,24,32,40,48,56},{2,10,18,26,34,42,50,58},{4,12,20,28,36,44,52,6..., dimensions={0} | all-to-all | bytes 2031616 | tf_op jit(solution)/shard_map/all_to_all | solution.py:52
  58.6 0.9 copy-done.1
  59.5 0.4 totals.1
  59.9 44.4 %all_to_all.27.got2 = bf16[8,1424,128]{2,1,0:T(8,128)(2,1)S(1)} all-to-all(bf16[8,1424,128]{2,1,0:T(8,128)(2,1)S(1)} %totals.1), channel_id=1, replica_groups={{0,64,128,192,256,320,384,448},{2,66,130,194,258,322,386,450},{4,68,132..., dimensions={0} | all-to-all | bytes 5832704 | tf_op jit(solution)/shard_map/all_to_all | solution.py:52
  104.3 6.5 %attention.1 = bf16[8,400,128]{2,1,0:T(8,128)(2,1)S(1)} custom-call(bf16[8,496,128]{2,1,0:T(8,128)(2,1)S(1)} %all_to_all.26.got1, bf16[8,1424,128]{2,1,0:T(8,128)(2,1)S(1)} %all_to_all.27.got2), custom_call_target="tpu_custom_call" | custom-call | flops 4300000256 | bytes 4000000 | tf_op jit(solution)/shard_map/attention/pallas_call | solution.py:278
  110.8 18.0 %all_to_all.28.got3 = bf16[8,400,128]{2,1,0:T(8,128)(2,1)S(1)} all-to-all(bf16[8,400,128]{2,1,0:T(8,128)(2,1)S(1)} %attention.1), channel_id=1, replica_groups={{0,8,16,24,32,40,48,56},{2,10,18,26,34,42,50,58},{4,12,20,28,36,44,52,6..., dimensions={0} | all-to-all | bytes 1638400 | tf_op jit(solution)/shard_map/all_to_all | solution.py:52
  128.8 6.0 %collective-permute-start.2 = (bf16[8,64,128]{2,1,0:T(8,128)(2,1)S(1)}, bf16[8,64,128]{2,1,0:T(8,128)(2,1)S(1)}, u32[]{:S(2)}, u32[]{:S(2)}) collective-permute-start(bf16[8,64,128]{2,1,0:T(8,128)(2,1)S(1)} %slice.4), channel_id=1, source_target_pairs={{0,1},{1,0},{2,3},{3,2},{4,5},{5,4},{6,7},{7,6},{8,9},{9,8},{10,11... | collective-permute-start | bytes 393224 | tf_op jit(solution)/shard_map/ppermute | solution.py:56
  134.8 1.0 collective-permute-done.2.sent
  135.8 1.6 %output.1 = (f32[4,32,2048]{2,1,0:T(8,128)S(1)}, bf16[4,32,2048]{2,1,0:T(8,128)(2,1)S(1)}) custom-call(bf16[8,1424,128]{2,1,0:T(8,128)(2,1)S(1)} %all_to_all.27.got2, bf16[8,400,128]{2,1,0:T(8,128)(2,1)S(1)} %all_to_all.28.got3, bf16[8,64,128]{2,1,0:T(8,128)(2,1)S(1)} %collective-permute-done.2.sent, bf16[256,256]{1,0:T(8,128)(2,1)S(1)} %copy-done.2, ...), custom_call_target="tpu_custom_call" | custom-call | flops 400000000 | bytes 4000000 | tf_op jit(solution)/shard_map/output/pallas_call | solution.py:278
  137.3 2.3 %collective-permute-start.3 = (bf16[4,32,2048]{2,1,0:T(8,128)(2,1)S(1)}, bf16[4,32,2048]{2,1,0:T(8,128)(2,1)S(1)}, u32[]{:S(2)}, u32[]{:S(2)}) collective-permute-start(bf16[4,32,2048]{2,1,0:T(8,128)(2,1)S(1)} %get-tuple-element.18), channel_id=1, source_target_pairs={{0,1},{1,0},{2,3},{3,2},{4,5},{5,4},{6,7},{7,6},{8,9},{9,8},{10,11... | collective-permute-start | bytes 1572872 | tf_op jit(solution)/shard_map/ppermute | solution.py:56
  139.6 1.5 collective-permute-done.3
  141.2 0.1 add_convert_fusion
  141.3 11.6 %all_to_all.29 = bf16[4,32,2048]{2,1,0:T(8,128)(2,1)S(1)} all-to-all(bf16[4,32,2048]{2,1,0:T(8,128)(2,1)S(1)} %add_convert_fusion), channel_id=1, replica_groups=mesh['z'=8,'y'=8,'x'=4,'c'=2] {'x'}, dimensions={0} | all-to-all | bytes 1048576 | tf_op jit(solution)/shard_map/all_to_all | solution.py:329
  152.9 0.7 reduce_sum.12
  (9 shorter events, 0.0 us)
Async XLA Ops:
  12.5 9.2 %copy-start.3 = (bf16[4,32,2048]{2,1,0:T(8,128)(2,1)}, bf16[4,32,2048]{2,1,0:T(8,128)(2,1)S(1)}, u32[]{:S(2)}) copy-start(bf16[4,32,2048]{2,1,0:T(8,128)(2,1)S(1)} %all_to_all.25.refs_0_) | copy-start | bytes 1572868
  12.5 9.2 %collective-permute-start = (bf16[4,32,2048]{2,1,0:T(8,128)(2,1)S(1)}, bf16[4,32,2048]{2,1,0:T(8,128)(2,1)S(1)}, u32[]{:S(2)}, u32[]{:S(2)}) collective-permute-start(bf16[4,32,2048]{2,1,0:T(8,128)(2,1)S(1)} %all_to_all.25.refs_0_), channel_id=1, source_target_pairs={{0,1},{1,0},{2,3},{3,2},{4,5},{5,4},{6,7},{7,6},{8,9},{9,8},{10,11... | collective-permute-start | bytes 1572872 | tf_op jit(solution)/shard_map/ppermute | solution.py:56
  21.7 0.8 copy-start.4
  29.3 3.5 %collective-permute-start.1 = (bf16[8,64,128]{2,1,0:T(8,128)(2,1)}, bf16[8,64,128]{2,1,0:T(8,128)(2,1)S(1)}, u32[]{:S(2)}, u32[]{:S(2)}) collective-permute-start(bf16[8,64,128]{2,1,0:T(8,128)(2,1)} %get-tuple-element.13), channel_id=1, source_target_pairs={{0,1},{1,0},{2,3},{3,2},{4,5},{5,4},{6,7},{7,6},{8,9},{9,8},{10,11... | collective-permute-start | bytes 393224 | tf_op jit(solution)/shard_map/ppermute | solution.py:56
  58.6 0.9 copy-start.1
  104.3 31.5 %copy-start = (f32[256,256]{1,0:T(8,128)S(1)}, f32[256,256]{1,0:T(8,128)}, u32[]{:S(2)}) copy-start(f32[256,256]{1,0:T(8,128)} %get-tuple-element.16.inner) | copy-start | bytes 786436
  104.3 31.5 %copy-start.2 = (bf16[256,256]{1,0:T(8,128)(2,1)S(1)}, bf16[256,256]{1,0:T(8,128)(2,1)}, u32[]{:S(2)}) copy-start(bf16[256,256]{1,0:T(8,128)(2,1)} %get-tuple-element.15.qrot) | copy-start | bytes 393220
  128.8 6.9 %collective-permute-start.2 = (bf16[8,64,128]{2,1,0:T(8,128)(2,1)S(1)}, bf16[8,64,128]{2,1,0:T(8,128)(2,1)S(1)}, u32[]{:S(2)}, u32[]{:S(2)}) collective-permute-start(bf16[8,64,128]{2,1,0:T(8,128)(2,1)S(1)} %slice.4), channel_id=1, source_target_pairs={{0,1},{1,0},{2,3},{3,2},{4,5},{5,4},{6,7},{7,6},{8,9},{9,8},{10,11... | collective-permute-start | bytes 393224 | tf_op jit(solution)/shard_map/ppermute | solution.py:56
  137.3 3.8 %collective-permute-start.3 = (bf16[4,32,2048]{2,1,0:T(8,128)(2,1)S(1)}, bf16[4,32,2048]{2,1,0:T(8,128)(2,1)S(1)}, u32[]{:S(2)}, u32[]{:S(2)}) collective-permute-start(bf16[4,32,2048]{2,1,0:T(8,128)(2,1)S(1)} %get-tuple-element.18), channel_id=1, source_target_pairs={{0,1},{1,0},{2,3},{3,2},{4,5},{5,4},{6,7},{7,6},{8,9},{9,8},{10,11... | collective-permute-start | bytes 1572872 | tf_op jit(solution)/shard_map/ppermute | solution.py:56

commit v4 on v3

--- a/solution.py
+++ b/solution.py
@@ -82,25 +82,28 @@
 
 
 def project_kernel(*refs):
-    own, other, wt = refs[:3]
-    far = refs[3:13]
-    m1, states, kvg, qrot, inner, xs = refs[13:19]
-    near = refs[19:29]
-    sems = refs[29]
-    copies = [pltpu.make_async_copy(src, dst, sems.at[k]) for k, (src, dst) in enumerate(zip(far, near))]
+    far, outs = refs[:13], refs[13:18]
+    near, made = refs[18:31], refs[31:36]
+    xs, in_sems, out_sems = refs[36:]
+    copies = [pltpu.make_async_copy(src, dst, in_sems.at[k]) for k, (src, dst) in enumerate(zip(far, near))]
     for copy in copies:
         copy.start()
-    gain, wrk, wrv, row_turn, run_turn, wrq, wfq, wfk, wfv, gates = near
+    own, gain, other, wrk, wrv, row_turn, run_turn, gates, wfq, wt, wrq, wfk, wfv = near
+    m1, states, kvg, qrot, inner = made
+    stores = [pltpu.make_async_copy(src, dst, out_sems.at[k]) for k, (src, dst) in enumerate(zip(made, outs))]
     place, _, _, c = places()
     rate = of_head(RATES, lax.axis_index("x") * 2 + c)
     copies[0].wait()
-    for j in range(4):
-        for part, side in ((own, c), (other, 1 - c)):
+    copies[1].wait()
+    for part, side in ((own, c), (other, 1 - c)):
+        if part is other:
+            copies[2].wait()
+        for j in range(4):
             x = part[j].astype(F32)
             scaled = x * lax.rsqrt(jnp.mean(x * x, axis=1, keepdims=True) + eps) * gain[...]
             xs[pl.ds(pl.multiple_of(64 * j + 32 * side, 32), 32), :] = scaled.astype(BF)
     x = xs[...]
-    for copy in copies[1:5]:
+    for copy in copies[3:7]:
         copy.wait()
     cos_run = run_turn[0, pl.ds(place, 1), :]
     sin_run = run_turn[1, pl.ds(place, 1), :]
@@ -125,16 +128,10 @@
             states[j, 32 * half : 32 * half + 32, :] = piece
             m1[j, SA0 + 32 * half : SA0 + 32 * half + 32, :] = piece
             m1[j, SB0 + 32 * half : SB0 + 32 * half + 32, :] = piece
-    for copy in copies[5:]:
+    stores[1].start()
+    for copy in copies[7:10]:
         copy.wait()
-    rq = turned(dot(x, wrq[...]).astype(BF).astype(F32), 1.0).astype(BF)
-    qrot[...] = rq
-    spread = row - col
-    within = jnp.where(spread >= 0, jnp.exp(-rate * jnp.maximum(spread, 0).astype(F32)), 0.0)
-    inner[...] = dot((dot_nt(rq, rk) * within).astype(BF), rv)
     fq = dot(x, wfq[...]).astype(BF)
-    kvg[K0 : K0 + RUN, :] = dot(x, wfk[...]).astype(BF)
-    kvg[V0 : V0 + RUN, :] = dot(x, wfv[...]).astype(BF)
     line = lax.broadcasted_iota(jnp.int32, (16, LANES), 0)
     gate = jnp.where(line < 8, gates[0:1, :], gates[1:2, :]) * (FOX**0.5)
     high = gate.astype(BF).astype(F32)
@@ -145,12 +142,27 @@
     of_query = jnp.where(slot < 3, third, jnp.where(slot < 6, 1.0, 0.0)).astype(BF)
     third = jnp.where(slot == 3, high, jnp.where(slot == 4, middle, low))
     of_key = jnp.where(slot < 3, 1.0, jnp.where(slot < 6, -third, 0.0)).astype(BF)
-    kvg[KG0 : KG0 + 16, :] = of_key
     for j in range(N):
         m1[j, Q0 : Q0 + RUN, :] = fq
         m1[j, QG0 : QG0 + 16, :] = of_query
         for k in range(3):
             m1[j, W0 + 32 * k : W0 + 32 * k + 32, :] = wt[k]
+    stores[0].start()
+    for copy in copies[10:]:
+        copy.wait()
+    kvg[KG0 : KG0 + 16, :] = of_key
+    kvg[K0 : K0 + RUN, :] = dot(x, wfk[...]).astype(BF)
+    kvg[V0 : V0 + RUN, :] = dot(x, wfv[...]).astype(BF)
+    stores[2].start()
+    rq = turned(dot(x, wrq[...]).astype(BF).astype(F32), 1.0).astype(BF)
+    qrot[...] = rq
+    stores[3].start()
+    spread = row - col
+    within = jnp.where(spread >= 0, jnp.exp(-rate * jnp.maximum(spread, 0).astype(F32)), 0.0)
+    inner[...] = dot((dot_nt(rq, rk) * within).astype(BF), rv)
+    stores[4].start()
+    for store in stores:
+        store.wait()
 
 
 def totals_kernel(got1, kvg, m2):
@@ -273,13 +285,13 @@
     return [pl.BlockSpec(memory_space=pltpu.VMEM)] * count
 
 
-def call(kernel, outs, scratch, args, flops, nbytes, name, limit, far=()):
+def call(kernel, outs, scratch, args, flops, nbytes, name, limit, far=(), out_space=pltpu.VMEM):
     specs = vmem(len(args)) + [pl.BlockSpec(memory_space=pltpu.HBM)] * len(far)
     return pl.pallas_call(
         kernel,
         out_shape=outs,
         in_specs=specs,
-        out_specs=vmem(len(outs)),
+        out_specs=[pl.BlockSpec(memory_space=out_space)] * len(outs),
         scratch_shapes=scratch,
         cost_estimate=pl.CostEstimate(flops=flops, bytes_accessed=nbytes, transcendentals=0),
         compiler_params=pltpu.CompilerParams(vmem_limit_bytes=limit << 20),
@@ -298,14 +310,16 @@
     other = swapped(own)
     wt = jnp.concatenate([w_out_ret, w_out_fox], axis=0).reshape(3, LANES, 32).transpose(0, 2, 1)
     far = (
-        gain.reshape(1, 2048), w_ret_k, w_ret_v, jnp.asarray(ROW_TURN), jnp.asarray(RUN_TURN),
-        w_ret_q, w_fox_q, w_fox_k, w_fox_v, fox_gates.reshape(2, LANES),
-    )
+        own, gain.reshape(1, 2048), other, w_ret_k, w_ret_v, jnp.asarray(ROW_TURN), jnp.asarray(RUN_TURN),
+        fox_gates.reshape(2, LANES), w_fox_q, wt, w_ret_q, w_fox_k, w_fox_v,
+    )
+    made = [struct(N, R1, LANES), struct(N, 64, LANES), struct(KG0 + 16, LANES), struct(RUN, RET), struct(RUN, RET, dtype=F32)]
     m1, states, kvg, qrot, inner = call(
         project_kernel,
-        [struct(N, R1, LANES), struct(N, 64, LANES), struct(KG0 + 16, LANES), struct(RUN, RET), struct(RUN, RET, dtype=F32)],
-        [pltpu.VMEM((RUN, 2048), BF)] + [pltpu.VMEM(a.shape, a.dtype) for a in far] + [pltpu.SemaphoreType.DMA((len(far),))],
-        (own, other, wt), 1_400_000_000, 8_000_000, "project", 60, far,
+        made,
+        [pltpu.VMEM(a.shape, a.dtype) for a in (*far, *made)]
+        + [pltpu.VMEM((RUN, 2048), BF), pltpu.SemaphoreType.DMA((len(far),)), pltpu.SemaphoreType.DMA((len(made),))],
+        (), 1_400_000_000, 8_000_000, "project", 60, far, pltpu.HBM,
     )
     m1 = lax.dynamic_update_slice(m1, swapped(states), (0, SB0, 0))
     got1 = exchanged(m1, GROUPS_A)

time: 154 us -> 153 us (level)
  no operation moved by 1% of the time
where the time goes in v4:
time: 153 us
  blocking collectives  111 us (73%)
  starting transfers between devices  18.2 us (12%)
  Pallas kernels  14.2 us (9%)
  waiting for transfers between devices  3.83 us (3%)
  local copies, waits for them, and re-layouts  3.37 us (2%)
  other arithmetic  2.19 us (1%)
    all_to_all x3, blocking collectives, exchanged(): lax.all_to_all(message, ALL, 0, 0, axis_index_groups=groups, tiled=True)  87.6 us
    ppermute x4, starting transfers between devices, swapped(): return lax.ppermute(array, 'c', [(0, 1), (1, 0)])  18.2 us
    pallas_call x4, Pallas kernels, call(): pl.pallas_call(kernel, out_shape=outs, in_specs=specs, out_specs=[pl.Bloc...  14.2 us
    all_to_all x1, blocking collectives, per_device(): lax.all_to_all(pair, 'x', 0, 0, tiled=True).astype(F32)  11.6 us
    all_to_all x1, blocking collectives, per_device(): lax.all_to_all(jnp.broadcast_to(tokens[None], (4, 32, 2048)), 'x', 0, 0,...  11.6 us
    ppermute x4, waiting for transfers between devices, swapped(): return lax.ppermute(array, 'c', [(0, 1), (1, 0)])  3.83 us
  transfers between devices with their start and end apart: 4, of which 4 were waited for; matrix products, arithmetic and copies ran while one was open for 1% of the time, Pallas kernels for 0%

profile of v4, /device:TPU:1, one launch (start us, length us, event | category | flops | bytes accessed | tf_op | source)
XLA Modules:
  0.0 152.6 jit_solution(14911459007389358781)
XLA Ops:
  0.0 0.9 broadcast_in_dim.2
  1.0 11.6 %all_to_all.25.refs_0_ = bf16[4,32,2048]{2,1,0:T(8,128)(2,1)S(1)} all-to-all(bf16[4,32,2048]{2,1,0:T(8,128)(2,1)S(1)} %broadcast_in_dim.2), channel_id=1, replica_groups=mesh['z'=8,'y'=8,'x'=4,'c'=2] {'x'}, dimensions={0} | all-to-all | bytes 1048576 | tf_op jit(solution)/shard_map/all_to_all | solution.py:309
  12.5 7.7 %collective-permute-start = (bf16[4,32,2048]{2,1,0:T(8,128)(2,1)S(1)}, bf16[4,32,2048]{2,1,0:T(8,128)(2,1)S(1)}, u32[]{:S(2)}, u32[]{:S(2)}) collective-permute-start(bf16[4,32,2048]{2,1,0:T(8,128)(2,1)S(1)} %all_to_all.25.refs_0_), channel_id=1, source_target_pairs={{0,1},{1,0},{2,3},{3,2},{4,5},{5,4},{6,7},{7,6},{8,9},{9,8},{10,11... | collective-permute-start | bytes 1572872 | tf_op jit(solution)/shard_map/ppermute | solution.py:56
  20.2 1.3 bitcast_bitcast_fusion.refs_9_
  21.5 0.2 collective-permute-done.refs_2_
  21.7 0.8 copy-done.4
  22.5 5.8 %project.1 = (bf16[8,496,128]{2,1,0:T(8,128)(2,1)}, bf16[8,64,128]{2,1,0:T(8,128)(2,1)}, bf16[528,128]{1,0:T(8,128)(2,1)}, bf16[256,256]{1,0:T(8,128)(2,1)}, f32[256,256]{1,0:T(8,128)}) custom-call(bf16[4,32,2048]{2,1,0:T(8,128)(2,1)} %copy-done.3, f32[1,2048]{1,0:T(1,128)} %bitcast.9, bf16[4,32,2048]{2,1,0:T(8,128)(2,1)} %copy-done.4, ...), custom_call_target="tpu_custom_call" | custom-call | flops 1400000000 | bytes 8000000 | tf_op jit(solution)/shard_map/project/pallas_call | solution.py:290
  28.3 2.3 %collective-permute-start.1 = (bf16[8,64,128]{2,1,0:T(8,128)(2,1)}, bf16[8,64,128]{2,1,0:T(8,128)(2,1)S(1)}, u32[]{:S(2)}, u32[]{:S(2)}) collective-permute-start(bf16[8,64,128]{2,1,0:T(8,128)(2,1)} %get-tuple-element.13), channel_id=1, source_target_pairs={{0,1},{1,0},{2,3},{3,2},{4,5},{5,4},{6,7},{7,6},{8,9},{9,8},{10,11... | collective-permute-start | bytes 393224 | tf_op jit(solution)/shard_map/ppermute | solution.py:56
  30.6 1.2 collective-permute-done.1
  31.7 0.7 constant_dynamic-update-slice_fusion
  32.4 25.2 %all_to_all.26.got1 = bf16[8,496,128]{2,1,0:T(8,128)(2,1)S(1)} all-to-all(bf16[8,496,128]{2,1,0:T(8,128)(2,1)} %constant_dynamic-update-slice_fusion), channel_id=1, replica_groups={{0,8,16,24,32,40,48,56},{2,10,18,26,34,42,50,58},{4,12,20,28,36,44,52,6..., dimensions={0} | all-to-all | bytes 2031616 | tf_op jit(solution)/shard_map/all_to_all | solution.py:52
  57.6 0.9 copy-done.1
  58.5 0.4 totals.1
  58.9 44.4 %all_to_all.27.got2 = bf16[8,1424,128]{2,1,0:T(8,128)(2,1)S(1)} all-to-all(bf16[8,1424,128]{2,1,0:T(8,128)(2,1)S(1)} %totals.1), channel_id=1, replica_groups={{0,64,128,192,256,320,384,448},{2,66,130,194,258,322,386,450},{4,68,132..., dimensions={0} | all-to-all | bytes 5832704 | tf_op jit(solution)/shard_map/all_to_all | solution.py:52
  103.3 6.5 %attention.1 = bf16[8,400,128]{2,1,0:T(8,128)(2,1)S(1)} custom-call(bf16[8,496,128]{2,1,0:T(8,128)(2,1)S(1)} %all_to_all.26.got1, bf16[8,1424,128]{2,1,0:T(8,128)(2,1)S(1)} %all_to_all.27.got2), custom_call_target="tpu_custom_call" | custom-call | flops 4300000256 | bytes 4000000 | tf_op jit(solution)/shard_map/attention/pallas_call | solution.py:290
  109.8 18.0 %all_to_all.28.got3 = bf16[8,400,128]{2,1,0:T(8,128)(2,1)S(1)} all-to-all(bf16[8,400,128]{2,1,0:T(8,128)(2,1)S(1)} %attention.1), channel_id=1, replica_groups={{0,8,16,24,32,40,48,56},{2,10,18,26,34,42,50,58},{4,12,20,28,36,44,52,6..., dimensions={0} | all-to-all | bytes 1638400 | tf_op jit(solution)/shard_map/all_to_all | solution.py:52
  127.8 6.0 %collective-permute-start.2 = (bf16[8,64,128]{2,1,0:T(8,128)(2,1)S(1)}, bf16[8,64,128]{2,1,0:T(8,128)(2,1)S(1)}, u32[]{:S(2)}, u32[]{:S(2)}) collective-permute-start(bf16[8,64,128]{2,1,0:T(8,128)(2,1)S(1)} %slice.4), channel_id=1, source_target_pairs={{0,1},{1,0},{2,3},{3,2},{4,5},{5,4},{6,7},{7,6},{8,9},{9,8},{10,11... | collective-permute-start | bytes 393224 | tf_op jit(solution)/shard_map/ppermute | solution.py:56
  133.8 1.0 collective-permute-done.2.sent
  134.8 1.6 %output.1 = (f32[4,32,2048]{2,1,0:T(8,128)S(1)}, bf16[4,32,2048]{2,1,0:T(8,128)(2,1)S(1)}) custom-call(bf16[8,1424,128]{2,1,0:T(8,128)(2,1)S(1)} %all_to_all.27.got2, bf16[8,400,128]{2,1,0:T(8,128)(2,1)S(1)} %all_to_all.28.got3, bf16[8,64,128]{2,1,0:T(8,128)(2,1)S(1)} %collective-permute-done.2.sent, bf16[256,256]{1,0:T(8,128)(2,1)S(1)} %copy-done.2, ...), custom_call_target="tpu_custom_call" | custom-call | flops 400000000 | bytes 4000000 | tf_op jit(solution)/shard_map/output/pallas_call | solution.py:290
  136.4 2.3 %collective-permute-start.3 = (bf16[4,32,2048]{2,1,0:T(8,128)(2,1)S(1)}, bf16[4,32,2048]{2,1,0:T(8,128)(2,1)S(1)}, u32[]{:S(2)}, u32[]{:S(2)}) collective-permute-start(bf16[4,32,2048]{2,1,0:T(8,128)(2,1)S(1)} %get-tuple-element.18), channel_id=1, source_target_pairs={{0,1},{1,0},{2,3},{3,2},{4,5},{5,4},{6,7},{7,6},{8,9},{9,8},{10,11... | collective-permute-start | bytes 1572872 | tf_op jit(solution)/shard_map/ppermute | solution.py:56
  138.6 1.5 collective-permute-done.3
  140.2 0.1 add_convert_fusion
  140.3 11.6 %all_to_all.29 = bf16[4,32,2048]{2,1,0:T(8,128)(2,1)S(1)} all-to-all(bf16[4,32,2048]{2,1,0:T(8,128)(2,1)S(1)} %add_convert_fusion), channel_id=1, replica_groups=mesh['z'=8,'y'=8,'x'=4,'c'=2] {'x'}, dimensions={0} | all-to-all | bytes 1048576 | tf_op jit(solution)/shard_map/all_to_all | solution.py:343
  151.9 0.7 reduce_sum.12
  (9 shorter events, 0.0 us)
Async XLA Ops:
  12.5 9.2 %copy-start.3 = (bf16[4,32,2048]{2,1,0:T(8,128)(2,1)}, bf16[4,32,2048]{2,1,0:T(8,128)(2,1)S(1)}, u32[]{:S(2)}) copy-start(bf16[4,32,2048]{2,1,0:T(8,128)(2,1)S(1)} %all_to_all.25.refs_0_) | copy-start | bytes 1572868
  12.5 9.2 %collective-permute-start = (bf16[4,32,2048]{2,1,0:T(8,128)(2,1)S(1)}, bf16[4,32,2048]{2,1,0:T(8,128)(2,1)S(1)}, u32[]{:S(2)}, u32[]{:S(2)}) collective-permute-start(bf16[4,32,2048]{2,1,0:T(8,128)(2,1)S(1)} %all_to_all.25.refs_0_), channel_id=1, source_target_pairs={{0,1},{1,0},{2,3},{3,2},{4,5},{5,4},{6,7},{7,6},{8,9},{9,8},{10,11... | collective-permute-start | bytes 1572872 | tf_op jit(solution)/shard_map/ppermute | solution.py:56
  21.7 0.8 copy-start.4
  28.3 3.5 %collective-permute-start.1 = (bf16[8,64,128]{2,1,0:T(8,128)(2,1)}, bf16[8,64,128]{2,1,0:T(8,128)(2,1)S(1)}, u32[]{:S(2)}, u32[]{:S(2)}) collective-permute-start(bf16[8,64,128]{2,1,0:T(8,128)(2,1)} %get-tuple-element.13), channel_id=1, source_target_pairs={{0,1},{1,0},{2,3},{3,2},{4,5},{5,4},{6,7},{7,6},{8,9},{9,8},{10,11... | collective-permute-start | bytes 393224 | tf_op jit(solution)/shard_map/ppermute | solution.py:56
  57.6 0.9 copy-start.1
  103.3 31.5 %copy-start = (f32[256,256]{1,0:T(8,128)S(1)}, f32[256,256]{1,0:T(8,128)}, u32[]{:S(2)}) copy-start(f32[256,256]{1,0:T(8,128)} %get-tuple-element.16.inner) | copy-start | bytes 786436
  103.3 31.5 %copy-start.2 = (bf16[256,256]{1,0:T(8,128)(2,1)S(1)}, bf16[256,256]{1,0:T(8,128)(2,1)}, u32[]{:S(2)}) copy-start(bf16[256,256]{1,0:T(8,128)(2,1)} %get-tuple-element.15.qrot) | copy-start | bytes 393220
  127.8 7.0 %collective-permute-start.2 = (bf16[8,64,128]{2,1,0:T(8,128)(2,1)S(1)}, bf16[8,64,128]{2,1,0:T(8,128)(2,1)S(1)}, u32[]{:S(2)}, u32[]{:S(2)}) collective-permute-start(bf16[8,64,128]{2,1,0:T(8,128)(2,1)S(1)} %slice.4), channel_id=1, source_target_pairs={{0,1},{1,0},{2,3},{3,2},{4,5},{5,4},{6,7},{7,6},{8,9},{9,8},{10,11... | collective-permute-start | bytes 393224 | tf_op jit(solution)/shard_map/ppermute | solution.py:56
  136.4 3.8 %collective-permute-start.3 = (bf16[4,32,2048]{2,1,0:T(8,128)(2,1)S(1)}, bf16[4,32,2048]{2,1,0:T(8,128)(2,1)S(1)}, u32[]{:S(2)}, u32[]{:S(2)}) collective-permute-start(bf16[4,32,2048]{2,1,0:T(8,128)(2,1)S(1)} %get-tuple-element.18), channel_id=1, source_target_pairs={{0,1},{1,0},{2,3},{3,2},{4,5},{5,4},{6,7},{7,6},{8,9},{9,8},{10,11... | collective-permute-start | bytes 1572872 | tf_op jit(solution)/shard_map/ppermute | solution.py:56

commit v5 on v4

--- a/solution.py
+++ b/solution.py
@@ -20,9 +20,10 @@
 SP = ("z", "y")
 TP = ("x", "c")
 
-Q0, QG0, SA0, SB0, W0, R1 = 0, 256, 272, 336, 400, 496
-K0, V0, KG0, TA0, TB0, WW0, R2 = 0, 256, 512, 528, 592, 656, 1424
+Q0, QG0, SA0, SB0, W0, R1 = 0, 256, 272, 336, 400, 480
+K0, V0, KG0, TA0, TB0, WW0, R2 = 0, 256, 512, 528, 592, 656, 1312
 N0, D0, CA0, CB0, R3 = 0, 256, 272, 336, 400
+SPARE = 1296
 
 HEADS = np.arange(8, dtype=np.float64)
 RATES = np.where(HEADS < 4, 1.0 / (32.0 + 16.0 * HEADS), np.exp2(-(HEADS - 4)) / 16384.0)
@@ -126,11 +127,27 @@
         for half in range(2):
             piece = state[32 * j : 32 * j + 32, LANES * half : LANES * half + LANES]
             states[j, 32 * half : 32 * half + 32, :] = piece
-            m1[j, SA0 + 32 * half : SA0 + 32 * half + 32, :] = piece
-            m1[j, SB0 + 32 * half : SB0 + 32 * half + 32, :] = piece
-    stores[1].start()
     for copy in copies[7:10]:
         copy.wait()
+
+    @pl.when(c == 0)
+    def _():
+        for j in range(N):
+            m1[j, SA0 : SA0 + 64, :] = states[j]
+            m1[j, W0 : W0 + 32, :] = wt[0]
+            m1[j, W0 + 32 : W0 + 64, :] = wt[1]
+            m1[j, W0 + 64 : W0 + 80, :] = wt[2, 0:16, :]
+        states[0, 0:16, :] = wt[2, 16:32, :]
+
+    @pl.when(c == 1)
+    def _():
+        for j in range(N):
+            m1[j, SA0 : SA0 + 32, :] = wt[0]
+            m1[j, SA0 + 32 : SA0 + 64, :] = wt[1]
+            m1[j, W0 : W0 + 32, :] = wt[2]
+            m1[j, W0 + 32 : W0 + 80, :] = jnp.zeros((48, LANES), BF)
+
+    stores[1].start()
     fq = dot(x, wfq[...]).astype(BF)
     line = lax.broadcasted_iota(jnp.int32, (16, LANES), 0)
     gate = jnp.where(line < 8, gates[0:1, :], gates[1:2, :]) * (FOX**0.5)
@@ -145,8 +162,7 @@
     for j in range(N):
         m1[j, Q0 : Q0 + RUN, :] = fq
         m1[j, QG0 : QG0 + 16, :] = of_query
-        for k in range(3):
-            m1[j, W0 + 32 * k : W0 + 32 * k + 32, :] = wt[k]
+        m1[j, SB0 : SB0 + 64, :] = jnp.zeros((64, LANES), BF)
     stores[0].start()
     for copy in copies[10:]:
         copy.wait()
@@ -165,21 +181,35 @@
         store.wait()
 
 
-def totals_kernel(got1, kvg, m2):
-    head = lax.axis_index("x") * 2 + lax.axis_index("c")
-    sums = []
-    for start, which in ((SA0, head), (SB0, head ^ 1)):
-        decay = of_head(PER_RUN, which)
-        total = got1[0, start : start + 64, :].astype(F32)
-        for j in range(1, N):
-            total = total * decay + got1[j, start : start + 64, :].astype(F32)
-        sums.append(total.astype(BF))
+def totals_kernel(got1, kvg, spare, m2):
+    c = lax.axis_index("c")
+    head = lax.axis_index("x") * 2 + c
     for j in range(N):
         m2[j, 0 : KG0 + 16, :] = kvg[...]
-        m2[j, TA0 : TA0 + 64, :] = sums[0]
-        m2[j, TB0 : TB0 + 64, :] = sums[1]
-        for k in range(N):
-            m2[j, WW0 + 96 * k : WW0 + 96 * k + 96, :] = got1[k, W0 : W0 + 96, :]
+
+    @pl.when(c == 0)
+    def _():
+        sums = []
+        for start, which in ((SA0, head), (SB0, head ^ 1)):
+            decay = of_head(PER_RUN, which)
+            total = got1[0, start : start + 64, :].astype(F32)
+            for j in range(1, N):
+                total = total * decay + got1[j, start : start + 64, :].astype(F32)
+            sums.append(total.astype(BF))
+        for j in range(N):
+            m2[j, TA0 : TA0 + 64, :] = sums[0]
+            m2[j, TB0 : TB0 + 64, :] = sums[1]
+            for k in range(N):
+                m2[j, WW0 + 80 * k : WW0 + 80 * k + 80, :] = got1[k, W0 : W0 + 80, :]
+            m2[j, SPARE : SPARE + 16, :] = jnp.zeros((16, LANES), BF)
+
+    @pl.when(c == 1)
+    def _():
+        for j in range(N):
+            for k in range(N):
+                m2[j, TA0 + 96 * k : TA0 + 96 * k + 64, :] = got1[k, SA0 : SA0 + 64, :]
+                m2[j, TA0 + 96 * k + 64 : TA0 + 96 * k + 96, :] = got1[k, W0 : W0 + 32, :]
+            m2[j, SPARE : SPARE + 16, :] = spare[0, 0:16, :]
 
 
 def as_columns(rows, eye):
@@ -227,26 +257,55 @@
         return carry
 
     lax.fori_loop(0, N, one_run, 0, unroll=4)
-    for own, (sums, slices, carried) in enumerate(((TA0, SA0, CA0), (TB0, SB0, CB0))):
-        which = head ^ own
-        per_run, per_row = of_head(PER_RUN, which), of_head(PER_ROW, which)
-        state = jnp.zeros((64, LANES), F32)
-        for k in range(N):
-            state = jnp.where(k < b, state * per_row + got2[k, sums : sums + 64, :].astype(F32), state)
-        for j in range(N):
-            m3[j, carried : carried + 64, :] = state.astype(BF)
-            state = state * per_run + got1[j, slices : slices + 64, :].astype(F32)
+    @pl.when(c == 0)
+    def _():
+        for own, (sums, slices, carried) in enumerate(((TA0, SA0, CA0), (TB0, SB0, CB0))):
+            which = head ^ own
+            per_run, per_row = of_head(PER_RUN, which), of_head(PER_ROW, which)
+            state = jnp.zeros((64, LANES), F32)
+            for k in range(N):
+                state = jnp.where(k < b, state * per_row + got2[k, sums : sums + 64, :].astype(F32), state)
+            for j in range(N):
+                m3[j, carried : carried + 64, :] = state.astype(BF)
+                state = state * per_run + got1[j, slices : slices + 64, :].astype(F32)
+
+    @pl.when(c == 1)
+    def _():
+        for j in range(N):
+            for i in range(N):
+                m3[j, CA0 + 16 * i : CA0 + 16 * i + 16, :] = got2[i, SPARE : SPARE + 16, :]
 
 
 def output_kernel(got2, got3, sent, qrot, inner, keep, give, weight, mixed, state):
     _, _, _, c = places()
     rate = of_head(RATES, lax.axis_index("x") * 2 + c)
-    for i in range(N):
-        for k in range(N):
-            at = pl.multiple_of(jnp.where(c == 0, i * N + k, k * N + i) * 32, 32)
-            for h in range(3):
-                start = WW0 + 96 * k + 32 * h
-                weight[pl.ds(at, 32), LANES * h : LANES * h + LANES] = got2[i, start : start + 32, :]
+    @pl.when(c == 0)
+    def _():
+        for i in range(N):
+            for k in range(N):
+                at, start = (i * N + k) * 32, WW0 + 80 * k
+                weight[at : at + 32, :LANES] = got2[i, start : start + 32, :]
+                weight[at : at + 32, LANES : 2 * LANES] = got2[i, start + 32 : start + 64, :]
+                weight[at : at + 16, 2 * LANES :] = got2[i, start + 64 : start + 80, :]
+                at = (k * N + i) * 32
+                weight[at + 16 : at + 32, 2 * LANES :] = sent[k, 16 * i : 16 * i + 16, :]
+        for j in range(N):
+            for half in range(2):
+                piece = got3[j, CA0 + 32 * half : CA0 + 32 * half + 32, :]
+                state[32 * j : 32 * j + 32, LANES * half : LANES * half + LANES] = piece
+
+    @pl.when(c == 1)
+    def _():
+        for i in range(N):
+            for k in range(N):
+                at, start = (k * N + i) * 32, TA0 + 96 * k
+                for h in range(3):
+                    weight[at : at + 32, LANES * h : LANES * h + LANES] = got2[i, start + 32 * h : start + 32 * h + 32, :]
+        for j in range(N):
+            for half in range(2):
+                piece = sent[j, 64 + 32 * half : 64 + 32 * half + 32, :]
+                state[32 * j : 32 * j + 32, LANES * half : LANES * half + LANES] = piece
+
     num = got3[0, N0 : N0 + RUN, :].astype(F32)
     den = got3[0, D0 : D0 + 16, :].astype(F32)
     for j in range(1, N):
@@ -260,13 +319,6 @@
         raw = num[LANES * h : LANES * h + LANES] / column
         raw = raw * lax.rsqrt(jnp.mean(raw * raw, axis=1, keepdims=True) + eps)
         mixed[LANES * h : LANES * h + LANES, RET:] = raw.astype(BF)
-    for j in range(N):
-        for half in range(2):
-            start = 32 * half
-            piece = jnp.where(
-                c == 0, got3[j, CA0 + start : CA0 + start + 32, :].astype(F32), sent[j, start : start + 32, :].astype(F32)
-            )
-            state[32 * j : 32 * j + 32, LANES * half : LANES * half + LANES] = piece.astype(BF)
     steps = lax.broadcasted_iota(jnp.int32, (RUN, RET), 0)
     raw = inner[...] + dot(qrot[...], state[...]) * jnp.exp(-rate * (steps + 1).astype(F32))
     raw = raw * lax.rsqrt(jnp.mean(raw * raw, axis=1, keepdims=True) + eps)
@@ -321,9 +373,10 @@
         + [pltpu.VMEM((RUN, 2048), BF), pltpu.SemaphoreType.DMA((len(far),)), pltpu.SemaphoreType.DMA((len(made),))],
         (), 1_400_000_000, 8_000_000, "project", 60, far, pltpu.HBM,
     )
-    m1 = lax.dynamic_update_slice(m1, swapped(states), (0, SB0, 0))
+    spare = swapped(states)
+    m1 = lax.dynamic_update_slice(m1, spare, (0, SB0, 0))
     got1 = exchanged(m1, GROUPS_A)
-    (m2,) = call(totals_kernel, [struct(N, R2, LANES)], [], (got1, kvg), 1_000_000, 4_000_000, "totals", 16)
+    (m2,) = call(totals_kernel, [struct(N, R2, LANES)], [], (got1, kvg, spare), 1_000_000, 4_000_000, "totals", 16)
     got2 = exchanged(m2, GROUPS_B)
     (m3,) = call(
         attention_kernel,
@@ -332,7 +385,7 @@
         (got1, got2), 4_300_000_000, 4_000_000, "attention", 24,
     )
     got3 = exchanged(m3, GROUPS_A)
-    sent = swapped(got3[:, CB0 : CB0 + 64, :])
+    sent = swapped(got3[:, CA0 : CA0 + 128, :])
     keep, give = call(
         output_kernel,
         [struct(4, 32, 2048, dtype=F32), struct(4, 32, 2048)],

time: 153 us -> 151 us (0.987)
  blocking collectives: 111 us -> 108 us
    all_to_all x3, blocking collectives: 87.6 us -> 84.7 us  [exchanged(): lax.all_to_all(message, ALL, 0, 0, axis_index_groups=groups, tiled=True)]
where the time goes in v5:
time: 151 us; the launch traced here: 150 us
  blocking collectives  108 us (72%)
  starting transfers between devices  18.3 us (12%)
  Pallas kernels  14.3 us (9%)
  waiting for transfers between devices  4 us (3%)
  local copies, waits for them, and re-layouts  3.38 us (2%)
  other arithmetic  2.19 us (1%)
    all_to_all x3, blocking collectives, exchanged(): lax.all_to_all(message, ALL, 0, 0, axis_index_groups=groups, tiled=True)  84.7 us
    ppermute x4, starting transfers between devices, swapped(): return lax.ppermute(array, 'c', [(0, 1), (1, 0)])  18.3 us
    pallas_call x4, Pallas kernels, call(): pl.pallas_call(kernel, out_shape=outs, in_specs=specs, out_specs=[pl.Bloc...  14.3 us
    all_to_all x1, blocking collectives, per_device(): lax.all_to_all(pair, 'x', 0, 0, tiled=True).astype(F32)  11.6 us
    all_to_all x1, blocking collectives, per_device(): lax.all_to_all(jnp.broadcast_to(tokens[None], (4, 32, 2048)), 'x', 0, 0,...  11.6 us
    ppermute x4, waiting for transfers between devices, swapped(): return lax.ppermute(array, 'c', [(0, 1), (1, 0)])  4 us
  transfers between devices with their start and end apart: 4, of which 4 were waited for; matrix products, arithmetic and copies ran while one was open for 1% of the time, Pallas kernels for 0%

profile of v5, /device:TPU:1, one launch (start us, length us, event | category | flops | bytes accessed | tf_op | source)
XLA Modules:
  0.0 150.2 jit_solution(16647306391841656211)
XLA Ops:
  0.0 0.9 broadcast_in_dim.2
  1.0 11.6 %all_to_all.25.refs_0_ = bf16[4,32,2048]{2,1,0:T(8,128)(2,1)S(1)} all-to-all(bf16[4,32,2048]{2,1,0:T(8,128)(2,1)S(1)} %broadcast_in_dim.2), channel_id=1, replica_groups=mesh['z'=8,'y'=8,'x'=4,'c'=2] {'x'}, dimensions={0} | all-to-all | bytes 1048576 | tf_op jit(solution)/shard_map/all_to_all | solution.py:361
  12.5 7.7 %collective-permute-start = (bf16[4,32,2048]{2,1,0:T(8,128)(2,1)S(1)}, bf16[4,32,2048]{2,1,0:T(8,128)(2,1)S(1)}, u32[]{:S(2)}, u32[]{:S(2)}) collective-permute-start(bf16[4,32,2048]{2,1,0:T(8,128)(2,1)S(1)} %all_to_all.25.refs_0_), channel_id=1, source_target_pairs={{0,1},{1,0},{2,3},{3,2},{4,5},{5,4},{6,7},{7,6},{8,9},{9,8},{10,11... | collective-permute-start | bytes 1572872 | tf_op jit(solution)/shard_map/ppermute | solution.py:57
  20.2 1.3 bitcast_bitcast_fusion.refs_9_
  21.5 0.2 collective-permute-done.refs_2_
  21.7 0.8 copy-done.4
  22.5 5.8 %project.1 = (bf16[8,480,128]{2,1,0:T(8,128)(2,1)}, bf16[8,64,128]{2,1,0:T(8,128)(2,1)}, bf16[528,128]{1,0:T(8,128)(2,1)}, bf16[256,256]{1,0:T(8,128)(2,1)}, f32[256,256]{1,0:T(8,128)}) custom-call(bf16[4,32,2048]{2,1,0:T(8,128)(2,1)} %copy-done.3, f32[1,2048]{1,0:T(1,128)} %bitcast.9, bf16[4,32,2048]{2,1,0:T(8,128)(2,1)} %copy-done.4, ...), custom_call_target="tpu_custom_call" | custom-call | flops 1400000000 | bytes 8000000 | tf_op jit(solution)/shard_map/project/pallas_call | solution.py:342
  28.3 2.3 %collective-permute-start.1 = (bf16[8,64,128]{2,1,0:T(8,128)(2,1)}, bf16[8,64,128]{2,1,0:T(8,128)(2,1)S(1)}, u32[]{:S(2)}, u32[]{:S(2)}) collective-permute-start(bf16[8,64,128]{2,1,0:T(8,128)(2,1)} %get-tuple-element.13), channel_id=1, source_target_pairs={{0,1},{1,0},{2,3},{3,2},{4,5},{5,4},{6,7},{7,6},{8,9},{9,8},{10,11... | collective-permute-start | bytes 393224 | tf_op jit(solution)/shard_map/ppermute | solution.py:57
  30.6 1.2 collective-permute-done.1.spare
  31.8 0.7 constant_dynamic-update-slice_fusion
  32.5 24.8 %all_to_all.26.got1 = bf16[8,480,128]{2,1,0:T(8,128)(2,1)S(1)} all-to-all(bf16[8,480,128]{2,1,0:T(8,128)(2,1)} %constant_dynamic-update-slice_fusion), channel_id=1, replica_groups={{0,8,16,24,32,40,48,56},{2,10,18,26,34,42,50,58},{4,12,20,28,36,44,52,6..., dimensions={0} | all-to-all | bytes 1966080 | tf_op jit(solution)/shard_map/all_to_all | solution.py:53
  57.3 0.9 copy-done.1
  58.2 0.3 totals.1
  58.6 41.9 %all_to_all.27.got2 = bf16[8,1312,128]{2,1,0:T(8,128)(2,1)S(1)} all-to-all(bf16[8,1312,128]{2,1,0:T(8,128)(2,1)S(1)} %totals.1), channel_id=1, replica_groups={{0,64,128,192,256,320,384,448},{2,66,130,194,258,322,386,450},{4,68,132..., dimensions={0} | all-to-all | bytes 5373952 | tf_op jit(solution)/shard_map/all_to_all | solution.py:53
  100.5 6.5 %attention.1 = bf16[8,400,128]{2,1,0:T(8,128)(2,1)S(1)} custom-call(bf16[8,480,128]{2,1,0:T(8,128)(2,1)S(1)} %all_to_all.26.got1, bf16[8,1312,128]{2,1,0:T(8,128)(2,1)S(1)} %all_to_all.27.got2), custom_call_target="tpu_custom_call" | custom-call | flops 4300000256 | bytes 4000000 | tf_op jit(solution)/shard_map/attention/pallas_call | solution.py:342
  107.0 18.0 %all_to_all.28.got3 = bf16[8,400,128]{2,1,0:T(8,128)(2,1)S(1)} all-to-all(bf16[8,400,128]{2,1,0:T(8,128)(2,1)S(1)} %attention.1), channel_id=1, replica_groups={{0,8,16,24,32,40,48,56},{2,10,18,26,34,42,50,58},{4,12,20,28,36,44,52,6..., dimensions={0} | all-to-all | bytes 1638400 | tf_op jit(solution)/shard_map/all_to_all | solution.py:53
  125.0 6.1 %collective-permute-start.2 = (bf16[8,128,128]{2,1,0:T(8,128)(2,1)S(1)}, bf16[8,128,128]{2,1,0:T(8,128)(2,1)S(1)}, u32[]{:S(2)}, u32[]{:S(2)}) collective-permute-start(bf16[8,128,128]{2,1,0:T(8,128)(2,1)S(1)} %slice.4), channel_id=1, source_target_pairs={{0,1},{1,0},{2,3},{3,2},{4,5},{5,4},{6,7},{7,6},{8,9},{9,8},{10,11... | collective-permute-start | bytes 786440 | tf_op jit(solution)/shard_map/ppermute | solution.py:57
  131.1 1.1 collective-permute-done.2.sent
  132.2 1.7 %output.1 = (f32[4,32,2048]{2,1,0:T(8,128)S(1)}, bf16[4,32,2048]{2,1,0:T(8,128)(2,1)S(1)}) custom-call(bf16[8,1312,128]{2,1,0:T(8,128)(2,1)S(1)} %all_to_all.27.got2, bf16[8,400,128]{2,1,0:T(8,128)(2,1)S(1)} %all_to_all.28.got3, bf16[8,128,128]{2,1,0:T(8,128)(2,1)S(1)} %collective-permute-done.2.sent, bf16[256,256]{1,0:T(8,128)(2,1)S(1)} %copy-done.2, ...), custom_call_target="tpu_custom_call" | custom-call | flops 400000000 | bytes 4000000 | tf_op jit(solution)/shard_map/output/pallas_call | solution.py:342
  133.9 2.3 %collective-permute-start.3 = (bf16[4,32,2048]{2,1,0:T(8,128)(2,1)S(1)}, bf16[4,32,2048]{2,1,0:T(8,128)(2,1)S(1)}, u32[]{:S(2)}, u32[]{:S(2)}) collective-permute-start(bf16[4,32,2048]{2,1,0:T(8,128)(2,1)S(1)} %get-tuple-element.18), channel_id=1, source_target_pairs={{0,1},{1,0},{2,3},{3,2},{4,5},{5,4},{6,7},{7,6},{8,9},{9,8},{10,11... | collective-permute-start | bytes 1572872 | tf_op jit(solution)/shard_map/ppermute | solution.py:57
  136.2 1.5 %collective-permute-done.3 = bf16[4,32,2048]{2,1,0:T(8,128)(2,1)S(1)} collective-permute-done((bf16[4,32,2048]{2,1,0:T(8,128)(2,1)S(1)}, bf16[4,32,2048]{2,1,0:T(8,128)(2,1)S(1)}, u32[]{:S(2)}, u32[]{:S(2)}) %collective-permute-start.3) | collective-permute-done | bytes 524320 | tf_op jit(solution)/shard_map/ppermute | solution.py:57
  137.7 0.1 add_convert_fusion
  137.8 11.6 %all_to_all.29 = bf16[4,32,2048]{2,1,0:T(8,128)(2,1)S(1)} all-to-all(bf16[4,32,2048]{2,1,0:T(8,128)(2,1)S(1)} %add_convert_fusion), channel_id=1, replica_groups=mesh['z'=8,'y'=8,'x'=4,'c'=2] {'x'}, dimensions={0} | all-to-all | bytes 1048576 | tf_op jit(solution)/shard_map/all_to_all | solution.py:396
  149.4 0.7 reduce_sum.12
  (9 shorter events, 0.0 us)
Async XLA Ops:
  12.5 9.2 %copy-start.3 = (bf16[4,32,2048]{2,1,0:T(8,128)(2,1)}, bf16[4,32,2048]{2,1,0:T(8,128)(2,1)S(1)}, u32[]{:S(2)}) copy-start(bf16[4,32,2048]{2,1,0:T(8,128)(2,1)S(1)} %all_to_all.25.refs_0_) | copy-start | bytes 1572868
  12.5 9.2 %collective-permute-start = (bf16[4,32,2048]{2,1,0:T(8,128)(2,1)S(1)}, bf16[4,32,2048]{2,1,0:T(8,128)(2,1)S(1)}, u32[]{:S(2)}, u32[]{:S(2)}) collective-permute-start(bf16[4,32,2048]{2,1,0:T(8,128)(2,1)S(1)} %all_to_all.25.refs_0_), channel_id=1, source_target_pairs={{0,1},{1,0},{2,3},{3,2},{4,5},{5,4},{6,7},{7,6},{8,9},{9,8},{10,11... | collective-permute-start | bytes 1572872 | tf_op jit(solution)/shard_map/ppermute | solution.py:57
  21.7 0.8 copy-start.4
  28.3 3.5 %collective-permute-start.1 = (bf16[8,64,128]{2,1,0:T(8,128)(2,1)}, bf16[8,64,128]{2,1,0:T(8,128)(2,1)S(1)}, u32[]{:S(2)}, u32[]{:S(2)}) collective-permute-start(bf16[8,64,128]{2,1,0:T(8,128)(2,1)} %get-tuple-element.13), channel_id=1, source_target_pairs={{0,1},{1,0},{2,3},{3,2},{4,5},{5,4},{6,7},{7,6},{8,9},{9,8},{10,11... | collective-permute-start | bytes 393224 | tf_op jit(solution)/shard_map/ppermute | solution.py:57
  57.3 0.9 copy-start.1
  100.5 31.7 %copy-start = (f32[256,256]{1,0:T(8,128)S(1)}, f32[256,256]{1,0:T(8,128)}, u32[]{:S(2)}) copy-start(f32[256,256]{1,0:T(8,128)} %get-tuple-element.16.inner) | copy-start | bytes 786436
  100.5 31.7 %copy-start.2 = (bf16[256,256]{1,0:T(8,128)(2,1)S(1)}, bf16[256,256]{1,0:T(8,128)(2,1)}, u32[]{:S(2)}) copy-start(bf16[256,256]{1,0:T(8,128)(2,1)} %get-tuple-element.15.qrot) | copy-start | bytes 393220
  125.0 7.2 %collective-permute-start.2 = (bf16[8,128,128]{2,1,0:T(8,128)(2,1)S(1)}, bf16[8,128,128]{2,1,0:T(8,128)(2,1)S(1)}, u32[]{:S(2)}, u32[]{:S(2)}) collective-permute-start(bf16[8,128,128]{2,1,0:T(8,128)(2,1)S(1)} %slice.4), channel_id=1, source_target_pairs={{0,1},{1,0},{2,3},{3,2},{4,5},{5,4},{6,7},{7,6},{8,9},{9,8},{10,11... | collective-permute-start | bytes 786440 | tf_op jit(solution)/shard_map/ppermute | solution.py:57
  133.9 3.8 %collective-permute-start.3 = (bf16[4,32,2048]{2,1,0:T(8,128)(2,1)S(1)}, bf16[4,32,2048]{2,1,0:T(8,128)(2,1)S(1)}, u32[]{:S(2)}, u32[]{:S(2)}) collective-permute-start(bf16[4,32,2048]{2,1,0:T(8,128)(2,1)S(1)} %get-tuple-element.18), channel_id=1, source_target_pairs={{0,1},{1,0},{2,3},{3,2},{4,5},{5,4},{6,7},{7,6},{8,9},{9,8},{10,11... | collective-permute-start | bytes 1572872 | tf_op jit(solution)/shard_map/ppermute | solution.py:57

commit v6 on v5

--- a/solution.py
+++ b/solution.py
@@ -82,15 +82,22 @@
     return jnp.dot(left, right, preferred_element_type=F32)
 
 
+def turned(values, cosine, sine, scale):
+    first, second = values[:, :LANES], values[:, LANES:]
+    return jnp.concatenate(
+        [(first * cosine - second * sine) * scale, (first * sine + second * cosine) * scale], axis=1
+    )
+
+
 def project_kernel(*refs):
-    far, outs = refs[:13], refs[13:18]
-    near, made = refs[18:31], refs[31:36]
-    xs, in_sems, out_sems = refs[36:]
+    far, outs = refs[:10], refs[10:17]
+    near, made = refs[17:27], refs[27:34]
+    in_sems, out_sems = refs[34:]
     copies = [pltpu.make_async_copy(src, dst, in_sems.at[k]) for k, (src, dst) in enumerate(zip(far, near))]
     for copy in copies:
         copy.start()
-    own, gain, other, wrk, wrv, row_turn, run_turn, gates, wfq, wt, wrq, wfk, wfv = near
-    m1, states, kvg, qrot, inner = made
+    own, gain, other, wrk, wrv, row_turn, run_turn, gates, wfq, wt = near
+    m1, states, xs, turn, rkeys, rvalues, kgates = made
     stores = [pltpu.make_async_copy(src, dst, out_sems.at[k]) for k, (src, dst) in enumerate(zip(made, outs))]
     place, _, _, c = places()
     rate = of_head(RATES, lax.axis_index("x") * 2 + c)
@@ -103,6 +110,7 @@
             x = part[j].astype(F32)
             scaled = x * lax.rsqrt(jnp.mean(x * x, axis=1, keepdims=True) + eps) * gain[...]
             xs[pl.ds(pl.multiple_of(64 * j + 32 * side, 32), 32), :] = scaled.astype(BF)
+    stores[2].start()
     x = xs[...]
     for copy in copies[3:7]:
         copy.wait()
@@ -110,15 +118,15 @@
     sin_run = run_turn[1, pl.ds(place, 1), :]
     cosine = row_turn[0] * cos_run - row_turn[1] * sin_run
     sine = row_turn[1] * cos_run + row_turn[0] * sin_run
-
-    def turned(values, scale):
-        first, second = values[:, :LANES], values[:, LANES:]
-        return jnp.concatenate(
-            [(first * cosine - second * sine) * scale, (first * sine + second * cosine) * scale], axis=1
-        )
-
-    rk = turned(dot(x, wrk[...]).astype(BF).astype(F32), RET**-0.5).astype(BF)
+    turn[0] = cosine
+    turn[1] = sine
+    stores[3].start()
+    rk = turned(dot(x, wrk[...]).astype(BF).astype(F32), cosine, sine, RET**-0.5).astype(BF)
     rv = dot(x, wrv[...]).astype(BF)
+    rkeys[...] = rk
+    rvalues[...] = rv
+    stores[4].start()
+    stores[5].start()
     row = lax.broadcasted_iota(jnp.int32, (RUN, RET), 0)
     col = lax.broadcasted_iota(jnp.int32, (RUN, RET), 1)
     kd = (rk.astype(F32) * jnp.exp(-rate * (RUN - 1 - row).astype(F32))).astype(BF)
@@ -164,21 +172,24 @@
         m1[j, QG0 : QG0 + 16, :] = of_query
         m1[j, SB0 : SB0 + 64, :] = jnp.zeros((64, LANES), BF)
     stores[0].start()
-    for copy in copies[10:]:
-        copy.wait()
-    kvg[KG0 : KG0 + 16, :] = of_key
+    kgates[...] = of_key
+    stores[6].start()
+    for store in stores:
+        store.wait()
+
+
+def rest_kernel(xs, turn, rkeys, rvalues, kgates, wrq, wfk, wfv, kvg, qrot, inner):
+    rate = of_head(RATES, lax.axis_index("x") * 2 + lax.axis_index("c"))
+    x = xs[...]
+    kvg[KG0 : KG0 + 16, :] = kgates[...]
     kvg[K0 : K0 + RUN, :] = dot(x, wfk[...]).astype(BF)
     kvg[V0 : V0 + RUN, :] = dot(x, wfv[...]).astype(BF)
-    stores[2].start()
-    rq = turned(dot(x, wrq[...]).astype(BF).astype(F32), 1.0).astype(BF)
+    rq = turned(dot(x, wrq[...]).astype(BF).astype(F32), turn[0], turn[1], 1.0).astype(BF)
     qrot[...] = rq
-    stores[3].start()
-    spread = row - col
+    row = lax.broadcasted_iota(jnp.int32, (RUN, RET), 0)
+    spread = row - lax.broadcasted_iota(jnp.int32, (RUN, RET), 1)
     within = jnp.where(spread >= 0, jnp.exp(-rate * jnp.maximum(spread, 0).astype(F32)), 0.0)
-    inner[...] = dot((dot_nt(rq, rk) * within).astype(BF), rv)
-    stores[4].start()
-    for store in stores:
-        store.wait()
+    inner[...] = dot((dot_nt(rq, rkeys[...]) * within).astype(BF), rvalues[...])
 
 
 def totals_kernel(got1, kvg, spare, m2):
@@ -256,7 +267,7 @@
         m3[j, D0 : D0 + 16, :] = jnp.where(line < 2, high, jnp.where(line < 4, den - high, 0.0)).astype(BF)
         return carry
 
-    lax.fori_loop(0, N, one_run, 0, unroll=4)
+    lax.fori_loop(0, N, one_run, 0, unroll=8)
     @pl.when(c == 0)
     def _():
         for own, (sums, slices, carried) in enumerate(((TA0, SA0, CA0), (TB0, SB0, CB0))):
@@ -363,19 +374,27 @@
     wt = jnp.concatenate([w_out_ret, w_out_fox], axis=0).reshape(3, LANES, 32).transpose(0, 2, 1)
     far = (
         own, gain.reshape(1, 2048), other, w_ret_k, w_ret_v, jnp.asarray(ROW_TURN), jnp.asarray(RUN_TURN),
-        fox_gates.reshape(2, LANES), w_fox_q, wt, w_ret_q, w_fox_k, w_fox_v,
-    )
-    made = [struct(N, R1, LANES), struct(N, 64, LANES), struct(KG0 + 16, LANES), struct(RUN, RET), struct(RUN, RET, dtype=F32)]
-    m1, states, kvg, qrot, inner = call(
+        fox_gates.reshape(2, LANES), w_fox_q, wt,
+    )
+    made = [
+        struct(N, R1, LANES), struct(N, 64, LANES), struct(RUN, 2048), struct(2, RUN, LANES, dtype=F32),
+        struct(RUN, RET), struct(RUN, RET), struct(16, LANES),
+    ]
+    m1, states, *passed = call(
         project_kernel,
         made,
         [pltpu.VMEM(a.shape, a.dtype) for a in (*far, *made)]
-        + [pltpu.VMEM((RUN, 2048), BF), pltpu.SemaphoreType.DMA((len(far),)), pltpu.SemaphoreType.DMA((len(made),))],
-        (), 1_400_000_000, 8_000_000, "project", 60, far, pltpu.HBM,
+        + [pltpu.SemaphoreType.DMA((len(far),)), pltpu.SemaphoreType.DMA((len(made),))],
+        (), 700_000_000, 8_000_000, "project", 60, far, pltpu.HBM,
     )
     spare = swapped(states)
     m1 = lax.dynamic_update_slice(m1, spare, (0, SB0, 0))
     got1 = exchanged(m1, GROUPS_A)
+    kvg, qrot, inner = call(
+        rest_kernel,
+        [struct(KG0 + 16, LANES), struct(RUN, RET), struct(RUN, RET, dtype=F32)],
+        [], (*passed, w_ret_q, w_fox_k, w_fox_v), 700_000_000, 4_000_000, "rest", 20,
+    )
     (m2,) = call(totals_kernel, [struct(N, R2, LANES)], [], (got1, kvg, spare), 1_000_000, 4_000_000, "totals", 16)
     got2 = exchanged(m2, GROUPS_B)
     (m3,) = call(

time: 151 us -> 149 us (0.987)
  blocking collectives: 108 us -> 83.1 us
  waiting for transfers between devices: 4 us -> 13 us
  starting transfers between devices: 18.3 us -> 26.1 us
  local copies, waits for them, and re-layouts: 3.38 us -> 10.2 us
    all_to_all x3 -> x2, blocking collectives: 84.7 us -> 59.9 us  [exchanged(): lax.all_to_all(message, ALL, 0, 0, axis_index_groups=groups, tiled=True)]
    all_to_all x0 -> x1, waiting for transfers between devices: none -> 8.98 us  [exchanged(): lax.all_to_all(message, ALL, 0, 0, axis_index_groups=groups, tiled=True)]
    all_to_all x0 -> x1, starting transfers between devices: none -> 7.78 us  [exchanged(): lax.all_to_all(message, ALL, 0, 0, axis_index_groups=groups, tiled=True)]
    unnamed x10 -> x28, local copies, waits for them, and re-layouts: 1.7 us -> 8.53 us
    pallas_call x4 -> x5, Pallas kernels: 14.3 us -> 13.9 us  [call(): pl.pallas_call(kernel, out_shape=outs, in_specs=specs, out_specs=[pl.Bloc...]
  transfers between devices with their start and end apart: 4 -> 5, of which waited for: 4 -> 5; matrix products, arithmetic and copies ran while one was open for 1% -> 1% of each run, Pallas kernels for 0% -> 1%
where the time goes in v6:
time: 149 us
  blocking collectives  83.1 us (56%)
  starting transfers between devices  26.1 us (18%)
  Pallas kernels  13.9 us (9%)
  waiting for transfers between devices  13 us (9%)
  local copies, waits for them, and re-layouts  10.2 us (7%)
  other arithmetic  2.18 us (1%)
    all_to_all x2, blocking collectives, exchanged(): lax.all_to_all(message, ALL, 0, 0, axis_index_groups=groups, tiled=True)  59.9 us
    ppermute x4, starting transfers between devices, swapped(): return lax.ppermute(array, 'c', [(0, 1), (1, 0)])  18.4 us
    pallas_call x5, Pallas kernels, call(): pl.pallas_call(kernel, out_shape=outs, in_specs=specs, out_specs=[pl.Bloc...  13.9 us
    all_to_all x1, blocking collectives, per_device(): lax.all_to_all(pair, 'x', 0, 0, tiled=True).astype(F32)  11.6 us
    all_to_all x1, blocking collectives, per_device(): lax.all_to_all(jnp.broadcast_to(tokens[None], (4, 32, 2048)), 'x', 0, 0,...  11.6 us
    all_to_all x1, waiting for transfers between devices, exchanged(): lax.all_to_all(message, ALL, 0, 0, axis_index_groups=groups, tiled=True)  8.98 us
    unnamed x28, local copies, waits for them, and re-layouts  8.53 us
    all_to_all x1, starting transfers between devices, exchanged(): lax.all_to_all(message, ALL, 0, 0, axis_index_groups=groups, tiled=True)  7.78 us
  transfers between devices with their start and end apart: 5, of which 5 were waited for; matrix products, arithmetic and copies ran while one was open for 1% of the time, Pallas kernels for 1%

profile of v6, /device:TPU:1, one launch (start us, length us, event | category | flops | bytes accessed | tf_op | source)
XLA Modules:
  0.0 148.7 jit_solution(9176561311742856319)
XLA Ops:
  0.0 0.9 broadcast_in_dim.2
  1.0 11.6 %all_to_all.25.refs_0_ = bf16[4,32,2048]{2,1,0:T(8,128)(2,1)S(1)} all-to-all(bf16[4,32,2048]{2,1,0:T(8,128)(2,1)S(1)} %broadcast_in_dim.2), channel_id=1, replica_groups=mesh['z'=8,'y'=8,'x'=4,'c'=2] {'x'}, dimensions={0} | all-to-all | bytes 1048576 | tf_op jit(solution)/shard_map/all_to_all | solution.py:372
  12.5 7.7 %collective-permute-start = (bf16[4,32,2048]{2,1,0:T(8,128)(2,1)S(1)}, bf16[4,32,2048]{2,1,0:T(8,128)(2,1)S(1)}, u32[]{:S(2)}, u32[]{:S(2)}) collective-permute-start(bf16[4,32,2048]{2,1,0:T(8,128)(2,1)S(1)} %all_to_all.25.refs_0_), channel_id=1, source_target_pairs={{0,1},{1,0},{2,3},{3,2},{4,5},{5,4},{6,7},{7,6},{8,9},{9,8},{10,11... | collective-permute-start | bytes 1572872 | tf_op jit(solution)/shard_map/ppermute | solution.py:57
  20.2 1.3 bitcast_bitcast_fusion.refs_9_
  22.5 4.5 %project.1 = (bf16[8,480,128]{2,1,0:T(8,128)(2,1)}, bf16[8,64,128]{2,1,0:T(8,128)(2,1)}, bf16[256,2048]{1,0:T(8,128)(2,1)}, f32[2,256,128]{2,1,0:T(8,128)}, bf16...) custom-call(bf16[4,32,2048]{2,1,0:T(8,128)(2,1)} %copy-done.12, f32[1,2048]{1,0:T(1,128)} %bitcast.9, ...), custom_call_target="tpu_custom_call" | custom-call | flops 700000000 | bytes 8000000 | tf_op jit(solution)/shard_map/project/pallas_call | solution.py:353
  27.1 2.4 %collective-permute-start.1 = (bf16[8,64,128]{2,1,0:T(8,128)(2,1)}, bf16[8,64,128]{2,1,0:T(8,128)(2,1)S(1)}, u32[]{:S(2)}, u32[]{:S(2)}) collective-permute-start(bf16[8,64,128]{2,1,0:T(8,128)(2,1)} %get-tuple-element.18), channel_id=1, source_target_pairs={{0,1},{1,0},{2,3},{3,2},{4,5},{5,4},{6,7},{7,6},{8,9},{9,8},{10,11... | collective-permute-start | bytes 393224 | tf_op jit(solution)/shard_map/ppermute | solution.py:57
  29.5 1.2 collective-permute-done.1.spare
  31.3 7.8 %all-to-all-start.1 = ((bf16[8,480,128]{2,1,0:T(8,128)(2,1)}), bf16[8,480,128]{2,1,0:T(8,128)(2,1)S(1)}, u32[]{:S(2)}, u32[]{:S(2)}) async-start(bf16[8,480,128]{2,1,0:T(8,128)(2,1)} %constant_dynamic-update-slice_fusion), calls=%async_computation.1 | async-start | bytes 1966080 | tf_op jit(solution)/shard_map/all_to_all | solution.py:53
  39.1 1.0 copy-done.2
  40.2 1.0 copy-done.3
  41.2 0.9 copy-done.4
  43.1 0.9 copy-done.10
  44.6 1.3 rest.1
  47.2 9.0 %all-to-all-done.1.got1 = bf16[8,480,128]{2,1,0:T(8,128)(2,1)S(1)} async-done(((bf16[8,480,128]{2,1,0:T(8,128)(2,1)}), bf16[8,480,128]{2,1,0:T(8,128)(2,1)S(1)}, u32[]{:S(2)}, u32[]{:S(2)}) %all-to-all-start.1) | async-done | bytes 983072 | tf_op jit(solution)/shard_map/all_to_all | solution.py:53
  56.2 0.9 copy-done.6
  57.5 41.9 %all_to_all.26.got2 = bf16[8,1312,128]{2,1,0:T(8,128)(2,1)S(1)} all-to-all(bf16[8,1312,128]{2,1,0:T(8,128)(2,1)S(1)} %totals.1), channel_id=1, replica_groups={{0,64,128,192,256,320,384,448},{2,66,130,194,258,322,386,450},{4,68,132..., dimensions={0} | all-to-all | bytes 5373952 | tf_op jit(solution)/shard_map/all_to_all | solution.py:53
  99.4 6.0 %attention.1 = bf16[8,400,128]{2,1,0:T(8,128)(2,1)S(1)} custom-call(bf16[8,480,128]{2,1,0:T(8,128)(2,1)S(1)} %all-to-all-done.1.got1, bf16[8,1312,128]{2,1,0:T(8,128)(2,1)S(1)} %all_to_all.26.got2), custom_call_target="tpu_custom_call" | custom-call | flops 4300000256 | bytes 4000000 | tf_op jit(solution)/shard_map/attention/pallas_call | solution.py:353
  105.5 18.0 %all_to_all.27.got3 = bf16[8,400,128]{2,1,0:T(8,128)(2,1)S(1)} all-to-all(bf16[8,400,128]{2,1,0:T(8,128)(2,1)S(1)} %attention.1), channel_id=1, replica_groups={{0,8,16,24,32,40,48,56},{2,10,18,26,34,42,50,58},{4,12,20,28,36,44,52,6..., dimensions={0} | all-to-all | bytes 1638400 | tf_op jit(solution)/shard_map/all_to_all | solution.py:53
  123.5 6.1 %collective-permute-start.2 = (bf16[8,128,128]{2,1,0:T(8,128)(2,1)S(1)}, bf16[8,128,128]{2,1,0:T(8,128)(2,1)S(1)}, u32[]{:S(2)}, u32[]{:S(2)}) collective-permute-start(bf16[8,128,128]{2,1,0:T(8,128)(2,1)S(1)} %slice.4), channel_id=1, source_target_pairs={{0,1},{1,0},{2,3},{3,2},{4,5},{5,4},{6,7},{7,6},{8,9},{9,8},{10,11... | collective-permute-start | bytes 786440 | tf_op jit(solution)/shard_map/ppermute | solution.py:57
  129.5 1.1 collective-permute-done.2.sent
  130.7 1.7 %output.1 = (f32[4,32,2048]{2,1,0:T(8,128)S(1)}, bf16[4,32,2048]{2,1,0:T(8,128)(2,1)S(1)}) custom-call(bf16[8,1312,128]{2,1,0:T(8,128)(2,1)S(1)} %all_to_all.26.got2, bf16[8,400,128]{2,1,0:T(8,128)(2,1)S(1)} %all_to_all.27.got3, bf16[8,128,128]{2,1,0:T(8,128)(2,1)S(1)} %collective-permute-done.2.sent, bf16[256,256]{1,0:T(8,128)(2,1)S(1)} %copy-done.8, ...), custom_call_target="tpu_custom_call" | custom-call | flops 400000000 | bytes 4000000 | tf_op jit(solution)/shard_map/output/pallas_call | solution.py:353
  132.4 2.3 %collective-permute-start.3 = (bf16[4,32,2048]{2,1,0:T(8,128)(2,1)S(1)}, bf16[4,32,2048]{2,1,0:T(8,128)(2,1)S(1)}, u32[]{:S(2)}, u32[]{:S(2)}) collective-permute-start(bf16[4,32,2048]{2,1,0:T(8,128)(2,1)S(1)} %get-tuple-element.28), channel_id=1, source_target_pairs={{0,1},{1,0},{2,3},{3,2},{4,5},{5,4},{6,7},{7,6},{8,9},{9,8},{10,11... | collective-permute-start | bytes 1572872 | tf_op jit(solution)/shard_map/ppermute | solution.py:57
  134.6 1.5 %collective-permute-done.3 = bf16[4,32,2048]{2,1,0:T(8,128)(2,1)S(1)} collective-permute-done((bf16[4,32,2048]{2,1,0:T(8,128)(2,1)S(1)}, bf16[4,32,2048]{2,1,0:T(8,128)(2,1)S(1)}, u32[]{:S(2)}, u32[]{:S(2)}) %collective-permute-start.3) | collective-permute-done | bytes 524320 | tf_op jit(solution)/shard_map/ppermute | solution.py:57
  136.3 11.6 %all_to_all.28 = bf16[4,32,2048]{2,1,0:T(8,128)(2,1)S(1)} all-to-all(bf16[4,32,2048]{2,1,0:T(8,128)(2,1)S(1)} %add_convert_fusion), channel_id=1, replica_groups=mesh['z'=8,'y'=8,'x'=4,'c'=2] {'x'}, dimensions={0} | all-to-all | bytes 1048576 | tf_op jit(solution)/shard_map/all_to_all | solution.py:415
  (29 shorter events, 5.8 us)
Async XLA Ops:
  12.5 9.2 %copy-start.12 = (bf16[4,32,2048]{2,1,0:T(8,128)(2,1)}, bf16[4,32,2048]{2,1,0:T(8,128)(2,1)S(1)}, u32[]{:S(2)}) copy-start(bf16[4,32,2048]{2,1,0:T(8,128)(2,1)S(1)} %all_to_all.25.refs_0_) | copy-start | bytes 1572868
  12.5 9.2 %collective-permute-start = (bf16[4,32,2048]{2,1,0:T(8,128)(2,1)S(1)}, bf16[4,32,2048]{2,1,0:T(8,128)(2,1)S(1)}, u32[]{:S(2)}, u32[]{:S(2)}) collective-permute-start(bf16[4,32,2048]{2,1,0:T(8,128)(2,1)S(1)} %all_to_all.25.refs_0_), channel_id=1, source_target_pairs={{0,1},{1,0},{2,3},{3,2},{4,5},{5,4},{6,7},{7,6},{8,9},{9,8},{10,11... | collective-permute-start | bytes 1572872 | tf_op jit(solution)/shard_map/ppermute | solution.py:57
  21.7 0.8 copy-start.13
  22.5 16.6 %copy-start = (bf16[2048,256]{1,0:T(8,128)(2,1)S(1)}, bf16[2048,256]{1,0:T(8,128)(2,1)}, u32[]{:S(2)}) copy-start(bf16[2048,256]{1,0:T(8,128)(2,1)} %wrq.1) | copy-start | bytes 3145732
  27.0 12.1 %copy-start.1 = (bf16[256,2048]{1,0:T(8,128)(2,1)S(1)}, bf16[256,2048]{1,0:T(8,128)(2,1)}, u32[]{:S(2)}) copy-start(bf16[256,2048]{1,0:T(8,128)(2,1)} %get-tuple-element.19.xs) | copy-start | bytes 3145732
  27.1 3.6 %collective-permute-start.1 = (bf16[8,64,128]{2,1,0:T(8,128)(2,1)}, bf16[8,64,128]{2,1,0:T(8,128)(2,1)S(1)}, u32[]{:S(2)}, u32[]{:S(2)}) collective-permute-start(bf16[8,64,128]{2,1,0:T(8,128)(2,1)} %get-tuple-element.18), channel_id=1, source_target_pairs={{0,1},{1,0},{2,3},{3,2},{4,5},{5,4},{6,7},{7,6},{8,9},{9,8},{10,11... | collective-permute-start | bytes 393224 | tf_op jit(solution)/shard_map/ppermute | solution.py:57
  31.3 24.9 %all-to-all-start.1 = ((bf16[8,480,128]{2,1,0:T(8,128)(2,1)}), bf16[8,480,128]{2,1,0:T(8,128)(2,1)S(1)}, u32[]{:S(2)}, u32[]{:S(2)}) async-start(bf16[8,480,128]{2,1,0:T(8,128)(2,1)} %constant_dynamic-update-slice_fusion), calls=%async_computation.1 | async-start | bytes 1966080 | tf_op jit(solution)/shard_map/all_to_all | solution.py:53
  39.1 1.0 copy-start.2
  40.2 1.0 copy-start.3
  41.2 0.9 copy-start.4
  42.2 0.9 copy-start.9
  43.1 0.9 copy-start.10
  44.0 0.7 copy-start.11
  45.9 0.7 copy-start.5
  46.6 0.7 copy-start.7
  56.2 0.9 copy-start.6
  99.4 31.3 %copy-start.8 = (bf16[256,256]{1,0:T(8,128)(2,1)S(1)}, bf16[256,256]{1,0:T(8,128)(2,1)}, u32[]{:S(2)}) copy-start(bf16[256,256]{1,0:T(8,128)(2,1)} %copy-done.7) | copy-start | bytes 393220
  123.5 7.2 %collective-permute-start.2 = (bf16[8,128,128]{2,1,0:T(8,128)(2,1)S(1)}, bf16[8,128,128]{2,1,0:T(8,128)(2,1)S(1)}, u32[]{:S(2)}, u32[]{:S(2)}) collective-permute-start(bf16[8,128,128]{2,1,0:T(8,128)(2,1)S(1)} %slice.4), channel_id=1, source_target_pairs={{0,1},{1,0},{2,3},{3,2},{4,5},{5,4},{6,7},{7,6},{8,9},{9,8},{10,11... | collective-permute-start | bytes 786440 | tf_op jit(solution)/shard_map/ppermute | solution.py:57
  132.4 3.8 %collective-permute-start.3 = (bf16[4,32,2048]{2,1,0:T(8,128)(2,1)S(1)}, bf16[4,32,2048]{2,1,0:T(8,128)(2,1)S(1)}, u32[]{:S(2)}, u32[]{:S(2)}) collective-permute-start(bf16[4,32,2048]{2,1,0:T(8,128)(2,1)S(1)} %get-tuple-element.28), channel_id=1, source_target_pairs={{0,1},{1,0},{2,3},{3,2},{4,5},{5,4},{6,7},{7,6},{8,9},{9,8},{10,11... | collective-permute-start | bytes 1572872 | tf_op jit(solution)/shard_map/ppermute | solution.py:57

commit v7 on v6

--- a/solution.py
+++ b/solution.py
@@ -287,7 +287,7 @@
                 m3[j, CA0 + 16 * i : CA0 + 16 * i + 16, :] = got2[i, SPARE : SPARE + 16, :]
 
 
-def output_kernel(got2, got3, sent, qrot, inner, keep, give, weight, mixed, state):
+def output_kernel(got2, got3, sent, qrot, inner, give, weight, mixed, state):
     _, _, _, c = places()
     rate = of_head(RATES, lax.axis_index("x") * 2 + c)
     @pl.when(c == 0)
@@ -334,14 +334,21 @@
     raw = inner[...] + dot(qrot[...], state[...]) * jnp.exp(-rate * (steps + 1).astype(F32))
     raw = raw * lax.rsqrt(jnp.mean(raw * raw, axis=1, keepdims=True) + eps)
     mixed[:, :RET] = raw.astype(BF)
-    for side, target in ((c, keep), (1 - c, give)):
-        rows = jnp.concatenate(
-            [mixed[pl.ds(pl.multiple_of(64 * j + 32 * side, 32), 32), :] for j in range(4)], axis=0
-        )
-        for n in range(4):
-            part = dot_nt(rows, weight[512 * n : 512 * n + 512, :])
-            for j in range(4):
-                target[j, :, 512 * n : 512 * n + 512] = part[32 * j : 32 * j + 32].astype(target.dtype)
+    half_product(mixed, weight, 1 - c, give)
+
+
+def half_product(mixed, weight, side, target):
+    rows = jnp.concatenate(
+        [mixed[pl.ds(pl.multiple_of(64 * j + 32 * side, 32), 32), :] for j in range(4)], axis=0
+    )
+    for n in range(4):
+        part = dot_nt(rows, weight[512 * n : 512 * n + 512, :])
+        for j in range(4):
+            target[j, :, 512 * n : 512 * n + 512] = part[32 * j : 32 * j + 32].astype(target.dtype)
+
+
+def keep_kernel(mixed, weight, keep):
+    half_product(mixed, weight, lax.axis_index("c"), keep)
 
 
 def vmem(count):
@@ -405,13 +412,17 @@
     )
     got3 = exchanged(m3, GROUPS_A)
     sent = swapped(got3[:, CA0 : CA0 + 128, :])
-    keep, give = call(
+    give, weight, mixed = call(
         output_kernel,
-        [struct(4, 32, 2048, dtype=F32), struct(4, 32, 2048)],
-        [pltpu.VMEM((2048, 384), BF), pltpu.VMEM((RUN, 384), BF), pltpu.VMEM((RET, RET), BF)],
-        (got2, got3, sent, qrot, inner), 400_000_000, 4_000_000, "output", 20,
-    )
-    pair = (keep + swapped(give).astype(F32)).astype(BF)
+        [struct(4, 32, 2048), struct(2048, 384), struct(RUN, 384)],
+        [pltpu.VMEM((RET, RET), BF)],
+        (got2, got3, sent, qrot, inner), 300_000_000, 4_000_000, "output", 20,
+    )
+    given = swapped(give)
+    (keep,) = call(
+        keep_kernel, [struct(4, 32, 2048, dtype=F32)], [], (mixed, weight), 200_000_000, 3_000_000, "keep", 8,
+    )
+    pair = (keep + given.astype(F32)).astype(BF)
     return jnp.sum(lax.all_to_all(pair, "x", 0, 0, tiled=True).astype(F32), axis=0).astype(BF)
 
 

time: 149 us -> 149 us (level)
    pallas_call x5 -> x6, Pallas kernels: 13.9 us -> 14 us  [call(): pl.pallas_call(kernel, out_shape=outs, in_specs=specs, out_specs=[pl.Bloc...]
where the time goes in v7:
time: 149 us; the launch traced here: 148 us
  blocking collectives  83.1 us (56%)
  starting transfers between devices  26.2 us (18%)
  Pallas kernels  14 us (9%)
  waiting for transfers between devices  12.4 us (8%)
  local copies, waits for them, and re-layouts  10.2 us (7%)
  other arithmetic  2.18 us (1%)
    all_to_all x2, blocking collectives, exchanged(): lax.all_to_all(message, ALL, 0, 0, axis_index_groups=groups, tiled=True)  59.9 us
    ppermute x4, starting transfers between devices, swapped(): return lax.ppermute(array, 'c', [(0, 1), (1, 0)])  18.4 us
    pallas_call x6, Pallas kernels, call(): pl.pallas_call(kernel, out_shape=outs, in_specs=specs, out_specs=[pl.Bloc...  14 us
    all_to_all x1, blocking collectives, per_device(): lax.all_to_all(pair, 'x', 0, 0, tiled=True).astype(F32)  11.6 us
    all_to_all x1, blocking collectives, per_device(): lax.all_to_all(jnp.broadcast_to(tokens[None], (4, 32, 2048)), 'x', 0, 0,...  11.6 us
    all_to_all x1, waiting for transfers between devices, exchanged(): lax.all_to_all(message, ALL, 0, 0, axis_index_groups=groups, tiled=True)  8.98 us
    unnamed x28, local copies, waits for them, and re-layouts  8.53 us
    all_to_all x1, starting transfers between devices, exchanged(): lax.all_to_all(message, ALL, 0, 0, axis_index_groups=groups, tiled=True)  7.78 us
  transfers between devices with their start and end apart: 5, of which 5 were waited for; matrix products, arithmetic and copies ran while one was open for 1% of the time, Pallas kernels for 1%

profile of v7, /device:TPU:1, one launch (start us, length us, event | category | flops | bytes accessed | tf_op | source)
XLA Modules:
  0.0 148.1 jit_solution(2835706556361803204)
XLA Ops:
  0.0 0.9 broadcast_in_dim.2
  1.0 11.6 %all_to_all.25.refs_0_ = bf16[4,32,2048]{2,1,0:T(8,128)(2,1)S(1)} all-to-all(bf16[4,32,2048]{2,1,0:T(8,128)(2,1)S(1)} %broadcast_in_dim.2), channel_id=1, replica_groups=mesh['z'=8,'y'=8,'x'=4,'c'=2] {'x'}, dimensions={0} | all-to-all | bytes 1048576 | tf_op jit(solution)/shard_map/all_to_all | solution.py:379
  12.5 7.7 %collective-permute-start = (bf16[4,32,2048]{2,1,0:T(8,128)(2,1)S(1)}, bf16[4,32,2048]{2,1,0:T(8,128)(2,1)S(1)}, u32[]{:S(2)}, u32[]{:S(2)}) collective-permute-start(bf16[4,32,2048]{2,1,0:T(8,128)(2,1)S(1)} %all_to_all.25.refs_0_), channel_id=1, source_target_pairs={{0,1},{1,0},{2,3},{3,2},{4,5},{5,4},{6,7},{7,6},{8,9},{9,8},{10,11... | collective-permute-start | bytes 1572872 | tf_op jit(solution)/shard_map/ppermute | solution.py:57
  20.2 1.3 bitcast_bitcast_fusion.refs_9_
  22.5 4.5 %project.1 = (bf16[8,480,128]{2,1,0:T(8,128)(2,1)}, bf16[8,64,128]{2,1,0:T(8,128)(2,1)}, bf16[256,2048]{1,0:T(8,128)(2,1)}, f32[2,256,128]{2,1,0:T(8,128)}, bf16...) custom-call(bf16[4,32,2048]{2,1,0:T(8,128)(2,1)} %copy-done.12, f32[1,2048]{1,0:T(1,128)} %bitcast.9, ...), custom_call_target="tpu_custom_call" | custom-call | flops 700000000 | bytes 8000000 | tf_op jit(solution)/shard_map/project/pallas_call | solution.py:360
  27.1 2.4 %collective-permute-start.1 = (bf16[8,64,128]{2,1,0:T(8,128)(2,1)}, bf16[8,64,128]{2,1,0:T(8,128)(2,1)S(1)}, u32[]{:S(2)}, u32[]{:S(2)}) collective-permute-start(bf16[8,64,128]{2,1,0:T(8,128)(2,1)} %get-tuple-element.19), channel_id=1, source_target_pairs={{0,1},{1,0},{2,3},{3,2},{4,5},{5,4},{6,7},{7,6},{8,9},{9,8},{10,11... | collective-permute-start | bytes 393224 | tf_op jit(solution)/shard_map/ppermute | solution.py:57
  29.5 1.2 collective-permute-done.1.spare
  31.3 7.8 %all-to-all-start.1 = ((bf16[8,480,128]{2,1,0:T(8,128)(2,1)}), bf16[8,480,128]{2,1,0:T(8,128)(2,1)S(1)}, u32[]{:S(2)}, u32[]{:S(2)}) async-start(bf16[8,480,128]{2,1,0:T(8,128)(2,1)} %constant_dynamic-update-slice_fusion), calls=%async_computation.1 | async-start | bytes 1966080 | tf_op jit(solution)/shard_map/all_to_all | solution.py:53
  39.1 1.0 copy-done.2
  40.2 1.0 copy-done.3
  41.2 0.9 copy-done.4
  42.2 0.9 copy-done.9
  43.1 0.9 copy-done.10
  44.6 1.3 rest.1
  47.2 9.0 %all-to-all-done.1.got1 = bf16[8,480,128]{2,1,0:T(8,128)(2,1)S(1)} async-done(((bf16[8,480,128]{2,1,0:T(8,128)(2,1)}), bf16[8,480,128]{2,1,0:T(8,128)(2,1)S(1)}, u32[]{:S(2)}, u32[]{:S(2)}) %all-to-all-start.1) | async-done | bytes 983072 | tf_op jit(solution)/shard_map/all_to_all | solution.py:53
  56.2 0.9 copy-done.6
  57.5 41.9 %all_to_all.26.got2 = bf16[8,1312,128]{2,1,0:T(8,128)(2,1)S(1)} all-to-all(bf16[8,1312,128]{2,1,0:T(8,128)(2,1)S(1)} %totals.1), channel_id=1, replica_groups={{0,64,128,192,256,320,384,448},{2,66,130,194,258,322,386,450},{4,68,132..., dimensions={0} | all-to-all | bytes 5373952 | tf_op jit(solution)/shard_map/all_to_all | solution.py:53
  99.4 6.0 %attention.1 = bf16[8,400,128]{2,1,0:T(8,128)(2,1)S(1)} custom-call(bf16[8,480,128]{2,1,0:T(8,128)(2,1)S(1)} %all-to-all-done.1.got1, bf16[8,1312,128]{2,1,0:T(8,128)(2,1)S(1)} %all_to_all.26.got2), custom_call_target="tpu_custom_call" | custom-call | flops 4300000256 | bytes 4000000 | tf_op jit(solution)/shard_map/attention/pallas_call | solution.py:360
  105.5 18.0 %all_to_all.27.got3 = bf16[8,400,128]{2,1,0:T(8,128)(2,1)S(1)} all-to-all(bf16[8,400,128]{2,1,0:T(8,128)(2,1)S(1)} %attention.1), channel_id=1, replica_groups={{0,8,16,24,32,40,48,56},{2,10,18,26,34,42,50,58},{4,12,20,28,36,44,52,6..., dimensions={0} | all-to-all | bytes 1638400 | tf_op jit(solution)/shard_map/all_to_all | solution.py:53
  123.5 6.1 %collective-permute-start.2 = (bf16[8,128,128]{2,1,0:T(8,128)(2,1)S(1)}, bf16[8,128,128]{2,1,0:T(8,128)(2,1)S(1)}, u32[]{:S(2)}, u32[]{:S(2)}) collective-permute-start(bf16[8,128,128]{2,1,0:T(8,128)(2,1)S(1)} %slice.4), channel_id=1, source_target_pairs={{0,1},{1,0},{2,3},{3,2},{4,5},{5,4},{6,7},{7,6},{8,9},{9,8},{10,11... | collective-permute-start | bytes 786440 | tf_op jit(solution)/shard_map/ppermute | solution.py:57
  129.5 1.1 collective-permute-done.2.sent
  130.7 1.2 output.1
  131.9 2.3 %collective-permute-start.3 = (bf16[4,32,2048]{2,1,0:T(8,128)(2,1)S(1)}, bf16[4,32,2048]{2,1,0:T(8,128)(2,1)S(1)}, u32[]{:S(2)}, u32[]{:S(2)}) collective-permute-start(bf16[4,32,2048]{2,1,0:T(8,128)(2,1)S(1)} %get-tuple-element.30), channel_id=1, source_target_pairs={{0,1},{1,0},{2,3},{3,2},{4,5},{5,4},{6,7},{7,6},{8,9},{9,8},{10,11... | collective-permute-start | bytes 1572872 | tf_op jit(solution)/shard_map/ppermute | solution.py:57
  135.8 11.6 %all_to_all.28 = bf16[4,32,2048]{2,1,0:T(8,128)(2,1)S(1)} all-to-all(bf16[4,32,2048]{2,1,0:T(8,128)(2,1)S(1)} %add_convert_fusion), channel_id=1, replica_groups=mesh['z'=8,'y'=8,'x'=4,'c'=2] {'x'}, dimensions={0} | all-to-all | bytes 1048576 | tf_op jit(solution)/shard_map/all_to_all | solution.py:426
  (30 shorter events, 6.4 us)
Async XLA Ops:
  12.5 9.2 %copy-start.12 = (bf16[4,32,2048]{2,1,0:T(8,128)(2,1)}, bf16[4,32,2048]{2,1,0:T(8,128)(2,1)S(1)}, u32[]{:S(2)}) copy-start(bf16[4,32,2048]{2,1,0:T(8,128)(2,1)S(1)} %all_to_all.25.refs_0_) | copy-start | bytes 1572868
  12.5 9.2 %collective-permute-start = (bf16[4,32,2048]{2,1,0:T(8,128)(2,1)S(1)}, bf16[4,32,2048]{2,1,0:T(8,128)(2,1)S(1)}, u32[]{:S(2)}, u32[]{:S(2)}) collective-permute-start(bf16[4,32,2048]{2,1,0:T(8,128)(2,1)S(1)} %all_to_all.25.refs_0_), channel_id=1, source_target_pairs={{0,1},{1,0},{2,3},{3,2},{4,5},{5,4},{6,7},{7,6},{8,9},{9,8},{10,11... | collective-permute-start | bytes 1572872 | tf_op jit(solution)/shard_map/ppermute | solution.py:57
  21.7 0.8 copy-start.13
  22.5 16.6 %copy-start = (bf16[2048,256]{1,0:T(8,128)(2,1)S(1)}, bf16[2048,256]{1,0:T(8,128)(2,1)}, u32[]{:S(2)}) copy-start(bf16[2048,256]{1,0:T(8,128)(2,1)} %wrq.1) | copy-start | bytes 3145732
  27.0 12.1 %copy-start.1 = (bf16[256,2048]{1,0:T(8,128)(2,1)S(1)}, bf16[256,2048]{1,0:T(8,128)(2,1)}, u32[]{:S(2)}) copy-start(bf16[256,2048]{1,0:T(8,128)(2,1)} %get-tuple-element.20.xs) | copy-start | bytes 3145732
  27.1 3.6 %collective-permute-start.1 = (bf16[8,64,128]{2,1,0:T(8,128)(2,1)}, bf16[8,64,128]{2,1,0:T(8,128)(2,1)S(1)}, u32[]{:S(2)}, u32[]{:S(2)}) collective-permute-start(bf16[8,64,128]{2,1,0:T(8,128)(2,1)} %get-tuple-element.19), channel_id=1, source_target_pairs={{0,1},{1,0},{2,3},{3,2},{4,5},{5,4},{6,7},{7,6},{8,9},{9,8},{10,11... | collective-permute-start | bytes 393224 | tf_op jit(solution)/shard_map/ppermute | solution.py:57
  31.3 24.9 %all-to-all-start.1 = ((bf16[8,480,128]{2,1,0:T(8,128)(2,1)}), bf16[8,480,128]{2,1,0:T(8,128)(2,1)S(1)}, u32[]{:S(2)}, u32[]{:S(2)}) async-start(bf16[8,480,128]{2,1,0:T(8,128)(2,1)} %constant_dynamic-update-slice_fusion), calls=%async_computation.1 | async-start | bytes 1966080 | tf_op jit(solution)/shard_map/all_to_all | solution.py:53
  39.1 1.0 copy-start.2
  40.2 1.0 copy-start.3
  41.2 0.9 copy-start.4
  42.2 0.9 copy-start.9
  43.1 0.9 copy-start.10
  44.0 0.7 copy-start.11
  45.9 0.7 copy-start.5
  46.6 0.7 copy-start.7
  56.2 0.9 copy-start.6
  99.4 31.3 %copy-start.8 = (bf16[256,256]{1,0:T(8,128)(2,1)S(1)}, bf16[256,256]{1,0:T(8,128)(2,1)}, u32[]{:S(2)}) copy-start(bf16[256,256]{1,0:T(8,128)(2,1)} %copy-done.7) | copy-start | bytes 393220
  123.5 7.2 %collective-permute-start.2 = (bf16[8,128,128]{2,1,0:T(8,128)(2,1)S(1)}, bf16[8,128,128]{2,1,0:T(8,128)(2,1)S(1)}, u32[]{:S(2)}, u32[]{:S(2)}) collective-permute-start(bf16[8,128,128]{2,1,0:T(8,128)(2,1)S(1)} %slice.4), channel_id=1, source_target_pairs={{0,1},{1,0},{2,3},{3,2},{4,5},{5,4},{6,7},{7,6},{8,9},{9,8},{10,11... | collective-permute-start | bytes 786440 | tf_op jit(solution)/shard_map/ppermute | solution.py:57
  131.9 3.8 %collective-permute-start.3 = (bf16[4,32,2048]{2,1,0:T(8,128)(2,1)S(1)}, bf16[4,32,2048]{2,1,0:T(8,128)(2,1)S(1)}, u32[]{:S(2)}, u32[]{:S(2)}) collective-permute-start(bf16[4,32,2048]{2,1,0:T(8,128)(2,1)S(1)} %get-tuple-element.30), channel_id=1, source_target_pairs={{0,1},{1,0},{2,3},{3,2},{4,5},{5,4},{6,7},{7,6},{8,9},{9,8},{10,11... | collective-permute-start | bytes 1572872 | tf_op jit(solution)/shard_map/ppermute | solution.py:57
